TPU v7x, 256 devices: a 4x2x16 block of a 4x16x16 slice. The times are simulated.
256 devices in a mesh: grp: 2 (over y), fs: 32 (over z, core), tp: 4 (over x).
Axes of the slice: x: 4, y: 2, z: 16, core: 2. Of those that a mesh axis runs over, the one named last changes fastest.
The devices are a block of a 4x16x16 slice.
Arguments:
- tokens: bfloat16 [24576, 4096], P(('grp', 'fs'), 'tp'), parts along dimension 0, may hold values from -1100 to 1100
- norm_gain: float32 [4096], P('fs'), may hold values from 0.1 to 1.9
- gate_master: float32 [32, 4096, 512], P(None, 'fs', 'tp'), may hold values from -0.09375 to 0.09375
- up_master: float32 [32, 4096, 512], P(None, 'fs', 'tp'), may hold values from -0.09375 to 0.09375
- down_master: float32 [32, 512, 4096], P(None, 'fs', 'tp'), may hold values from -0.25 to 0.25
- expert_ids: int32 [24576, 2], P(('grp', 'fs')), parts along dimension 0, may hold values from 0 to 31, as said below
- route_weights: float32 [24576, 2], P(('grp', 'fs')), parts along dimension 0, may hold values from 0.2 to 1
Outputs:
- gate_sampler: bfloat16 [64, 4096, 512], P(('grp', 'fs'), None, 'tp'), parts along dimension 0
- up_sampler: bfloat16 [64, 4096, 512], P(('grp', 'fs'), None, 'tp'), parts along dimension 0
- down_sampler: bfloat16 [64, 512, 4096], P(('grp', 'fs'), 'tp'), parts along dimension 0
- mixed: bfloat16 [24576, 4096], P(('grp', 'fs'), 'tp'), parts along dimension 0
There are 2 independent parts, one for each index of `grp`. A program takes and returns all parts, laid end to end along the dimension named above; an argument that names none is the same for every part. Nothing has to cross between parts.
Inputs may be any that keep to these rules, and one draw needn't show every extreme that they name: `expert_ids`: each row names two different experts of one group: experts g * 8 to (g + 1) * 8 - 1 for some g. In each aligned block of 384 rows every expert is named exactly 24 times.
All inputs are finite; a program needn't handle non-finite values.
Results may differ from a plain program's by a relative error of at most 0.0091.
Values may be sent and summed in bfloat16 or wider, within the bound.
A program may use at most 128 MiB of HBM per device.

v0:
```python
import jax
import jax.numpy as jnp
from jax import lax
from jax.sharding import Mesh
from jax.sharding import PartitionSpec as P

FS = ("fs_0", "fs_1")
GRP_FS = ("grp", "fs_0", "fs_1")


def sent_together(arrays, axis, split_dim, concat_dim, along):
    ends, at = ([], 0)
    for a in arrays[:-1]:
        at += a.shape[along]
        ends.append(at)
    both = jnp.concatenate(arrays, axis=along)
    return tuple(
        jnp.split(
            lax.all_to_all(both, axis, split_axis=split_dim, concat_axis=concat_dim, tiled=True),
            ends,
            axis=along,
        )
    )


def sent_to_all(shard, axis):
    copies = jnp.broadcast_to(shard, (lax.axis_size(axis), *shard.shape))
    return lax.all_to_all(copies, axis, split_axis=0, concat_axis=0, tiled=True)


def over_copies(shard, axis):
    everything = sent_to_all(shard, axis)
    return jnp.sum(everything, axis=0)


def cut_along(shard, dim, count):
    before, after = (shard.shape[:dim], shard.shape[dim + 1 :])
    return jnp.moveaxis(shard.reshape(*before, count, -1, *after), dim, 0)


def in_order(pieces, dim):
    pieces = jnp.moveaxis(pieces, 0, dim)
    shape = pieces.shape
    return pieces.reshape(*shape[:dim], shape[dim] * shape[dim + 1], *shape[dim + 2 :])


def moved_by_axis(pieces, axes, order):
    shape = [lax.axis_size(a) for a in axes]
    pieces = pieces.reshape(*shape, *pieces.shape[1:])
    for k in order:
        pieces = lax.all_to_all(pieces, axes[k], split_axis=k, concat_axis=k, tiled=True)
    return pieces.reshape(-1, *pieces.shape[len(axes) :])


def core_and_chips(shard, groups, order, split_dim, concat_dim):
    count = lax.axis_size(groups[0]) * lax.axis_size(groups[1])
    pieces = cut_along(shard, split_dim, count)
    return in_order(moved_by_axis(pieces, groups, order), concat_dim)


def shards(tokens, norm_gain, gate_master, up_master, down_master, expert_ids, route_weights):
    gain = norm_gain[None, :, None]
    gate_new = (gain * gate_master).astype(jnp.bfloat16)
    up_new = (gain * up_master).astype(jnp.bfloat16)
    gate_local, up_local = sent_together((gate_new, up_new), FS, 0, 1, 2)
    down_local = lax.all_to_all(
        lax.all_to_all(
            down_master.astype(jnp.bfloat16), FS, split_axis=0, concat_axis=1, tiled=True
        ),
        "tp",
        split_axis=1,
        concat_axis=2,
        tiled=True,
    )
    experts = lax.axis_size(FS)
    count = expert_ids.shape[0]
    top = expert_ids.shape[1]
    capacity = top * count // experts
    flat = expert_ids.reshape(-1)
    onehot = (flat[:, None] == jnp.arange(experts, dtype=jnp.int32)[None, :]).astype(jnp.int32)
    place = jnp.sum(jnp.cumsum(onehot, axis=0) * onehot, axis=1) - 1
    slots = flat * capacity + place
    owners = (
        jnp.zeros((experts * capacity,), jnp.int32)
        .at[slots]
        .set(jnp.arange(top * count, dtype=jnp.int32) // top)
    )
    values = tokens.astype(jnp.float32)
    squares = over_copies(jnp.sum(values * values, axis=1), "tp")
    width = tokens.shape[1] * lax.axis_size("tp")
    normed = (values * lax.rsqrt(squares / width + 1e-06)[:, None]).astype(jnp.bfloat16)
    outbound = normed[owners].reshape(experts, capacity, tokens.shape[1])
    arrived = lax.all_to_all(outbound, FS, split_axis=0, concat_axis=0, tiled=True).reshape(
        -1, tokens.shape[1]
    )
    piece = lax.all_gather(arrived, "tp", axis=1, tiled=True)
    gate_rows = gate_local[0]
    up_rows = up_local[0]
    gate = jnp.dot(piece, gate_rows, preferred_element_type=jnp.float32)
    up = jnp.dot(piece, up_rows, preferred_element_type=jnp.float32)
    hidden = (jax.nn.silu(gate) * up).astype(jnp.bfloat16)
    partial_value = jnp.dot(hidden, down_local[0], preferred_element_type=jnp.float32).astype(
        jnp.bfloat16
    )
    row_count = partial_value.shape[0]
    tp_count = lax.axis_size("tp")
    split_blocks = partial_value.reshape(row_count, tp_count, partial_value.shape[1] // tp_count)
    received = lax.all_to_all(split_blocks, "tp", split_axis=1, concat_axis=1, tiled=True)
    summed = jnp.sum(received.astype(jnp.float32), axis=1).astype(jnp.bfloat16)
    columns = summed.shape[1]
    returned = core_and_chips(
        summed.reshape(experts, capacity, columns), ("fs_0", "fs_1"), (1, 0), 0, 0
    )
    picked = (
        returned.reshape(experts * capacity, columns)[slots]
        .astype(jnp.float32)
        .reshape(count, top, columns)
    )
    mixed = jnp.sum(picked * route_weights[:, :, None], axis=1).astype(jnp.bfloat16)
    return (gate_local, up_local, down_local, mixed)


def solution(mesh):
    torus = Mesh(
        mesh.devices.reshape(mesh.shape["grp"], 16, 2, mesh.shape["tp"]),
        ("grp", "fs_0", "fs_1", "tp"),
    )
    return jax.shard_map(
        shards,
        mesh=torus,
        in_specs=(
            P(GRP_FS, "tp"),
            P(FS),
            P(None, FS, "tp"),
            P(None, FS, "tp"),
            P(None, FS, "tp"),
            P(GRP_FS, None),
            P(GRP_FS, None),
        ),
        out_specs=(
            P(GRP_FS, None, "tp"),
            P(GRP_FS, None, "tp"),
            P(GRP_FS, "tp", None),
            P(GRP_FS, "tp"),
        ),
        check_vma=False,
    )
```

profile of v0, /device:TPU:33, one launch (start us, length us, event | category | flops | bytes accessed | tf_op | source)
XLA Modules:
  0.0 508.7 jit_solution(12979693446361544687)
XLA Ops:
  7.2 1.4 fusion
  8.5 0.6 broadcast_in_dim.4
  9.1 5.1 %all-to-all-start.3 = ((f32[4,1,384]{2,1,0:T(1,128)}), f32[4,1,384]{2,1,0:T(1,128)S(1)}, u32[]{:S(2)}, u32[]{:S(2)}) async-start(f32[4,1,384]{2,1,0:T(1,128)} %broadcast_in_dim.4), calls=%async_computation.3 | async-start | bytes 12288 | tf_op jit(solution)/shard_map/all_to_all | solution.py:28
  14.3 2.7 convert_element_type.40
  17.0 1.4 all-to-all-done.3
  18.4 26.1 %all-to-all-start.1 = ((bf16[32,16,1024]{2,1,0:T(8,128)(2,1)}), bf16[32,16,1024]{2,1,0:T(8,128)(2,1)S(1)}, u32[]{:S(2)}, u32[]{:S(2)}) async-start(bf16[32,16,1024]{2,1,0:T(8,128)(2,1)} %convert_element_type.40), calls=%async_computation.1 | async-start | bytes 2097152 | tf_op jit(solution)/shard_map/all_to_all | solution.py:67
  44.5 0.1 copy.63
  44.7 0.1 eq.29
  44.8 0.1 eq.25
  45.0 1.7 reduce-window.6
  46.7 0.3 slice_reduce_fusion
  47.0 0.1 copy.62
  47.2 0.2 mul.67
  47.5 3.4 scatter_custom_fusion
  50.9 0.2 fusion.1
  51.1 3.6 gather_fusion
  54.7 45.3 %all-to-all-done.1 = bf16[32,16,1024]{2,1,0:T(8,128)(2,1)S(1)} async-done(((bf16[32,16,1024]{2,1,0:T(8,128)(2,1)}), bf16[32,16,1024]{2,1,0:T(8,128)(2,1)S(1)}, u32[]{:S(2)}, u32[]{:S(2)}) %all-to-all-start.1) | async-done | bytes 1048608 | tf_op jit(solution)/shard_map/all_to_all | solution.py:67
  100.0 5.1 %all-to-all-start.4 = ((bf16[32,24,1024]{2,1,0:T(8,128)(2,1)}), bf16[32,24,1024]{2,1,0:T(8,128)(2,1)}, u32[]{:S(2)}, u32[]{:S(2)}) async-start(bf16[32,24,1024]{2,1,0:T(8,128)(2,1)} %bitcast.5), calls=%async_computation.4 | async-start | bytes 3145728 | tf_op jit(solution)/shard_map/all_to_all | solution.py:93
  105.1 1.6 copy.80
  106.7 0.5 broadcast.107
  107.2 6.8 %reduce.6 = bf16[512,1024]{1,0:T(8,128)(2,1)S(1)} reduce(bf16[512,1,1024]{2,1,0:T(2,128)(2,1)S(1)} %bitcast.51, bf16[]{:T(256)} %broadcast.107), dimensions={1}, to_apply=%bitcast.43.reduce_sub_computation | reduce | bytes 2097154
  114.0 2.0 reshape.124
  116.0 66.9 %all-to-all-done.4 = bf16[32,24,1024]{2,1,0:T(8,128)(2,1)} async-done(((bf16[32,24,1024]{2,1,0:T(8,128)(2,1)}), bf16[32,24,1024]{2,1,0:T(8,128)(2,1)}, u32[]{:S(2)}, u32[]{:S(2)}) %all-to-all-start.4) | async-done | bytes 1572896 | tf_op jit(solution)/shard_map/all_to_all | solution.py:93
  182.9 3.6 all-to-all-start.2
  186.6 0.7 all-gather.2.cloned.1.call-update
  187.4 2.2 multiply_convert_fusion.1
  189.6 1.7 pad_maximum_fusion
  191.2 9.0 %all-to-all-done.2 = bf16[4,2,65536]{2,1,0:T(2,128)(2,1)S(1)} async-done(((bf16[4,2,65536]{2,1,0:T(2,128)(2,1)}), bf16[4,2,65536]{2,1,0:T(2,128)(2,1)S(1)}, u32[]{:S(2)}, u32[]{:S(2)}) %all-to-all-start.2) | async-done | bytes 1048608 | tf_op jit(solution)/shard_map/all_to_all | solution.py:66
  200.3 6.8 %all-to-all-start = ((bf16[32,128,256]{2,1,0:T(8,128)(2,1)}), bf16[32,128,256]{2,1,0:T(8,128)(2,1)}, u32[]{:S(2)}, u32[]{:S(2)}) async-start(bf16[32,128,256]{2,1,0:T(8,128)(2,1)} %pad_maximum_fusion), calls=%async_computation | async-start | bytes 4194304 | tf_op jit(solution)/shard_map/all_to_all | solution.py:19
  207.1 1.0 reshape.125
  208.0 0.4 copy.72
  208.4 0.7 copy.60
  209.1 98.2 %all-to-all-done = bf16[32,128,256]{2,1,0:T(8,128)(2,1)} async-done(((bf16[32,128,256]{2,1,0:T(8,128)(2,1)}), bf16[32,128,256]{2,1,0:T(8,128)(2,1)}, u32[]{:S(2)}, u32[]{:S(2)}) %all-to-all-start) | async-done | bytes 2097184 | tf_op jit(solution)/shard_map/all_to_all | solution.py:19
  307.3 1.7 fusion.23
  309.0 5.3 %fusion.5 = f32[768,128]{1,0:T(8,128)S(1)} fusion(bf16[768,4096]{1,0:T(8,128)(2,1)} %all-gather.2.cloned.1.call-done, bf16[1,4096,128]{2,1,0:T(8,128)(2,1)S(1)} %get-tuple-element.25), kind=kOutput, calls=%fused_computation.16 | convolution fusion | flops 805306368 | bytes 7733248 | tf_op jit(solution)/shard_map/dot_general | solution.py:99
  314.3 12.0 %convolution_convert_fusion = bf16[768,4096]{1,0:T(8,128)(2,1)} fusion(bf16[128,4096]{0,1:T(8,128)(2,1)S(1)} %bitcast.48, bf16[768,4096]{1,0:T(8,128)(2,1)} %all-gather.2.cloned.1.call-done, bf16[1,4096,128]{2,1,0:T(8,128)(2,1)S(1)} %get-tuple-element.24, f32[768,128]{1,0:T(8,128)S(1)} %fusion.5), kind=kOutput, calls=%fused_computation.3 | convolution fusion | flops 1614348288 | bytes 15073280 | tf_op jit(solution)/shard_map/dot_general | solution.py:102
  326.3 3.5 copy.79
  329.8 73.3 %all_to_all.68 = bf16[768,4,1024]{2,0,1:T(8,128)(2,1)} all-to-all(bf16[768,4,1024]{2,0,1:T(8,128)(2,1)S(1)} %bitcast.47), channel_id=1, replica_groups=mesh['grp'=2,'fs_0'=16,'fs_1'=2,'tp'=4] {'tp'}, dimensions={1} | all-to-all | bytes 12582912 | tf_op jit(solution)/shard_map/all_to_all | solution.py:108
  403.1 4.9 reduce_sum.51
  408.1 7.2 %all_to_all.69 = bf16[16,2,1,24,1024]{4,3,0,2,1:T(8,128)(2,1)S(1)} all-to-all(bf16[16,2,1,24,1024]{4,3,0,2,1:T(8,128)(2,1)S(1)} %copy.68), channel_id=1, replica_groups=mesh['grp'=2,'fs_0'=16,'fs_1'=2,'tp'=4] {'fs_1'}, dimensions={1} | all-to-all | bytes 3145728 | tf_op jit(solution)/shard_map/all_to_all | solution.py:51
  415.4 1.3 copy.69
  416.7 4.5 all-to-all-start.7
  421.2 0.1 copy.70
  421.4 1.3 copy.71
  422.7 67.3 %all-to-all-done.7 = bf16[16,2,1,24,1024]{4,3,1,2,0:T(8,128)(2,1)S(1)} async-done(((bf16[16,2,1,24,1024]{4,3,1,2,0:T(8,128)(2,1)}), bf16[16,2,1,24,1024]{4,3,1,2,0:T(8,128)(2,1)S(1)}, u32[]{:S(2)}, u32[]{:S(2)}) %all-to-all-start.7) | async-done | bytes 1572896 | tf_op jit(solution)/shard_map/all_to_all | solution.py:51
  490.0 3.6 gather_fusion.1
  493.6 3.4 reshape.94
  497.0 4.8 multiply_reduce_fusion
  (29 shorter events, 0.5 us)
Async XLA Ops:
  9.1 9.3 %all-to-all-start.3 = ((f32[4,1,384]{2,1,0:T(1,128)}), f32[4,1,384]{2,1,0:T(1,128)S(1)}, u32[]{:S(2)}, u32[]{:S(2)}) async-start(f32[4,1,384]{2,1,0:T(1,128)} %broadcast_in_dim.4), calls=%async_computation.3 | async-start | bytes 12288 | tf_op jit(solution)/shard_map/all_to_all | solution.py:28
  14.3 30.2 %copy-start.4 = (s32[384,2]{0,1:T(2,128)S(1)}, s32[384,2]{0,1:T(2,128)}, u32[]{:S(2)}) copy-start(s32[384,2]{0,1:T(2,128)} %param.12) | copy-start | bytes 9220
  17.0 33.9 %copy-start.1 = (bf16[384,1024]{1,0:T(8,128)(2,1)S(1)}, bf16[384,1024]{1,0:T(8,128)(2,1)}, u32[]{:S(2)}) copy-start(bf16[384,1024]{1,0:T(8,128)(2,1)} %param.7) | copy-start | bytes 2359300
  18.4 81.6 %all-to-all-start.1 = ((bf16[32,16,1024]{2,1,0:T(8,128)(2,1)}), bf16[32,16,1024]{2,1,0:T(8,128)(2,1)S(1)}, u32[]{:S(2)}, u32[]{:S(2)}) async-start(bf16[32,16,1024]{2,1,0:T(8,128)(2,1)} %convert_element_type.40), calls=%async_computation.1 | async-start | bytes 2097152 | tf_op jit(solution)/shard_map/all_to_all | solution.py:67
  100.0 82.9 %all-to-all-start.4 = ((bf16[32,24,1024]{2,1,0:T(8,128)(2,1)}), bf16[32,24,1024]{2,1,0:T(8,128)(2,1)}, u32[]{:S(2)}, u32[]{:S(2)}) async-start(bf16[32,24,1024]{2,1,0:T(8,128)(2,1)} %bitcast.5), calls=%async_computation.4 | async-start | bytes 3145728 | tf_op jit(solution)/shard_map/all_to_all | solution.py:93
  116.0 71.3 %copy-start.2 = (f32[32,128,128]{2,1,0:T(8,128)S(1)}, f32[32,128,128]{2,1,0:T(8,128)}, u32[]{:S(2)}) copy-start(f32[32,128,128]{2,1,0:T(8,128)} %param.9) | copy-start | bytes 6291460
  116.0 71.3 %copy-start.6 = (f32[128]{0:T(128)S(1)}, f32[128]{0:T(128)}, u32[]{:S(2)}) copy-start(f32[128]{0:T(128)} %param.8) | copy-start | bytes 1540
  182.9 17.3 %all-to-all-start.2 = ((bf16[4,2,65536]{2,1,0:T(2,128)(2,1)}), bf16[4,2,65536]{2,1,0:T(2,128)(2,1)S(1)}, u32[]{:S(2)}, u32[]{:S(2)}) async-start(bf16[4,2,65536]{2,1,0:T(2,128)(2,1)} %reshape.124), calls=%async_computation.2 | async-start | bytes 2097152 | tf_op jit(solution)/shard_map/all_to_all | solution.py:66
  186.5 122.5 %all-gather.2.cloned.1.call-start = ((), (), s32[]{:S(2)}) async-start(), calls=%async_computation.8 | async-start | bytes 7864320 | tf_op jit(solution)/shard_map/all_gather | solution.py:96
  200.3 107.0 %all-to-all-start = ((bf16[32,128,256]{2,1,0:T(8,128)(2,1)}), bf16[32,128,256]{2,1,0:T(8,128)(2,1)}, u32[]{:S(2)}, u32[]{:S(2)}) async-start(bf16[32,128,256]{2,1,0:T(8,128)(2,1)} %pad_maximum_fusion), calls=%async_computation | async-start | bytes 4194304 | tf_op jit(solution)/shard_map/all_to_all | solution.py:19
  309.0 5.3 %copy-start.3 = (bf16[1,4096,128]{2,1,0:T(8,128)(2,1)}, bf16[1,4096,128]{2,1,0:T(8,128)(2,1)S(1)}, u32[]{:S(2)}) copy-start(bf16[1,4096,128]{2,1,0:T(8,128)(2,1)S(1)} %get-tuple-element.25) | copy-start | bytes 3145732
  309.0 5.3 %copy-start = (bf16[1,4096,128]{2,1,0:T(8,128)(2,1)}, bf16[1,4096,128]{2,1,0:T(8,128)(2,1)S(1)}, u32[]{:S(2)}) copy-start(bf16[1,4096,128]{2,1,0:T(8,128)(2,1)S(1)} %get-tuple-element.24) | copy-start | bytes 3145732
  416.7 4.6 copy-start.5
  416.7 73.3 %all-to-all-start.7 = ((bf16[16,2,1,24,1024]{4,3,1,2,0:T(8,128)(2,1)}), bf16[16,2,1,24,1024]{4,3,1,2,0:T(8,128)(2,1)S(1)}, u32[]{:S(2)}, u32[]{:S(2)}) async-start(bf16[16,2,1,24,1024]{4,3,1,2,0:T(8,128)(2,1)} %copy.69), calls=%async_computation.7 | async-start | bytes 3145728 | tf_op jit(solution)/shard_map/all_to_all | solution.py:51
Sparse Core Ops, SparseCore 0:
  189.2 64.4 all-gather.1
where the time goes:
time: 512 us; the launch traced here: 509 us
  waiting for transfers between devices  289 us (56%)
  blocking collectives  80.5 us (16%)
  starting transfers between devices  51.3 us (10%)
  local copies, waits for them, and re-layouts  29.7 us (6%)
  other arithmetic  26.6 us (5%)
  matrix products  17.3 us (3%)
  between operations  14.4 us (3%)
    all_to_all x1, waiting for transfers between devices, sent_together(): lax.all_to_all(both, axis, split_axis=split_dim, concat_axis=concat_dim,...  98.2 us
    all_to_all x1, blocking collectives, shards(): lax.all_to_all(split_blocks, 'tp', split_axis=1, concat_axis=1, tiled=True)  73.3 us
    all_to_all x1, waiting for transfers between devices, moved_by_axis(): lax.all_to_all(pieces, axes[k], split_axis=k, concat_axis=k, tiled=True)  67.3 us
    all_to_all x1, waiting for transfers between devices, shards(): lax.all_to_all(outbound, FS, split_axis=0, concat_axis=0, tiled=True)  66.9 us
    all_to_all x1, waiting for transfers between devices, shards(): lax.all_to_all(down_master.astype(jnp.bfloat16), FS, split_axis=0, concat...  45.3 us
    all_to_all x1, starting transfers between devices, shards(): lax.all_to_all(down_master.astype(jnp.bfloat16), FS, split_axis=0, concat...  26.1 us
    dot_general x1, matrix products, shards(): jnp.dot(hidden, down_local[0], preferred_element_type=jnp.float32)  12 us
  transfers between devices with their start and end apart: 7, of which 6 were waited for; matrix products, arithmetic and copies ran while one was open for 6% of the time, Pallas kernels for 0%

commit v1 on v0

v1 whole, which is shorter than its diff:
```python
import functools

import jax
import jax.numpy as jnp
from jax import lax
from jax.experimental import pallas as pl
from jax.experimental.pallas import tpu as pltpu
from jax.sharding import PartitionSpec as P

MESH = pl.DeviceIdType.MESH
F32 = jnp.float32
BF16 = jnp.bfloat16
CHUNKS = 4


def peer_of(m, fs, half):
    rings = 2 * half
    z, core = fs // 2, fs % 2
    n = m // 2
    sign = 2 * (n % 2) - 1
    dz = (half - (n + 1) // 2) * sign
    other = 1 - m % 2
    peer = 2 * ((z + dz + rings) % rings) + (core + other) % 2
    inner = ((n + rings - 1) // rings) * (1 - n // (rings - 1))
    return peer, 2 * (n + sign * inner) + m % 2


def kernel(
    sizes,
    tok_h, gain_ref, gate_h, up_h, down_h, ids_ref, idst_ref, wts_ref,
    gate_o, up_o, down_o, mixed_o,
    tok, wf, df, ws, ds, gu, gc, dr, normed, xs, xr, x2, ps, pr, po, hr, rs, rt, rt2, sel, sq, mixed_v,
    load_sem, w_sem, d_sem, y_send, y_recv, g_send, g_recv, sq_send, sq_recv, t_send, t_recv,
    p_send, p_recv, h_send, h_recv, r_sem, o_sem, od_send, od_recv,
):
    experts, tps, rows, top, cap = sizes
    half = experts // 4
    per = experts // CHUNKS
    span = experts // tps
    fs, x, grp = lax.axis_index("fs"), lax.axis_index("tp"), lax.axis_index("grp")
    side = grp % 2
    partner = grp + 1 - 2 * side
    width = tok.shape[1]
    hcols = df.shape[2]
    my_cols = pl.ds(pl.multiple_of(side * hcols, hcols), hcols)

    def remote(src, dst, send, recv, where):
        return pltpu.make_async_remote_copy(
            src_ref=src, dst_ref=dst, send_sem=send, recv_sem=recv, device_id=where, device_id_type=MESH
        )

    first_peer, _ = peer_of(0, fs, half)

    def got(ref, sem):
        remote(ref, ref, sem, sem, {"fs": first_peer}).wait_recv()

    def sent(ref, sem):
        remote(ref, ref, sem, sem, {"fs": first_peer}).wait_send()

    def each_peer(fn):
        def step(m, _):
            peer, theirs = peer_of(m, fs, half)
            fn(m, peer, theirs)
            return 0

        lax.fori_loop(0, experts - 1, step, 0)

    def xpeer(j):
        return (x + j) % tps

    tok_load = pltpu.make_async_copy(tok_h, tok, load_sem.at[0])
    down_load = pltpu.make_async_copy(down_h.at[:, :, my_cols], df, load_sem.at[2])

    @pl.when(side == 0)
    def _():
        pltpu.make_async_copy(gate_h, wf, load_sem.at[1]).start()

    @pl.when(side == 1)
    def _():
        pltpu.make_async_copy(up_h, wf, load_sem.at[1]).start()

    down_load.start()
    tok_load.start()

    barrier = pltpu.get_barrier_semaphore()
    each_peer(
        lambda m, peer, theirs: pl.semaphore_signal(
            barrier, inc=1, device_id={"fs": peer}, device_id_type=MESH
        )
    )
    for j in range(1, tps):
        pl.semaphore_signal(barrier, inc=1, device_id={"tp": xpeer(j)}, device_id_type=MESH)
    pl.semaphore_signal(barrier, inc=1, device_id={"grp": partner}, device_id_type=MESH)

    pltpu.make_async_copy(gate_h, wf, load_sem.at[1]).wait()

    def cast_w(e, _):
        ws[e] = (gain_ref[...] * wf[e]).astype(BF16)
        return 0

    lax.fori_loop(0, experts, cast_w, 0)
    gu[side, fs] = ws[fs]
    pl.semaphore_wait(barrier, experts - 1 + tps - 1 + 1)

    each_peer(
        lambda m, peer, theirs: remote(
            ws.at[peer], gu.at[side, fs], w_sem.at[0], w_sem.at[1], {"fs": peer}
        ).start()
    )

    down_load.wait()

    def cast_d(e, _):
        ds[e] = df[e].astype(BF16)
        return 0

    lax.fori_loop(0, experts, cast_d, 0)
    dr[fs, :, my_cols] = ds[fs]
    tok_load.wait()
    values = tok[...].astype(F32)
    sq[0] = jnp.broadcast_to(jnp.sum(values * values, axis=1, keepdims=True), sq.shape[1:])

    each_peer(
        lambda m, peer, theirs: remote(
            ds.at[peer], dr.at[fs, :, my_cols], d_sem.at[0], d_sem.at[1], {"fs": peer}
        ).start()
    )
    for j in range(1, tps):
        remote(sq.at[0], sq.at[j], sq_send.at[j - 1], sq_recv.at[j - 1], {"tp": xpeer(j)}).start()

    block = per * cap
    e0 = lax.broadcasted_iota(jnp.int32, (experts, rows), 0)
    named = (idst_ref[0:1, :] == e0) | (idst_ref[1:2, :] == e0)
    before = lax.broadcasted_iota(jnp.int32, (rows, rows), 0) <= lax.broadcasted_iota(jnp.int32, (rows, rows), 1)
    count = jnp.dot(
        jnp.where(named, 1.0, 0.0).astype(BF16),
        jnp.where(before, 1.0, 0.0).astype(BF16),
        preferred_element_type=F32,
    )
    place = jnp.where(named, count, 0.0).astype(BF16)

    for j in range(1, tps):
        remote(sq.at[0], sq.at[j], sq_send.at[j - 1], sq_recv.at[j - 1], {"tp": xpeer(j)}).wait_recv()
    total_sq = sq[0][:, 0:1]
    for j in range(1, tps):
        total_sq = total_sq + sq[j][:, 0:1]
    scale = lax.rsqrt(total_sq / (width * tps) + 1e-06)
    normed[...] = (tok[...].astype(F32) * scale).astype(BF16)

    for b in range(CHUNKS):
        slot = lax.broadcasted_iota(jnp.int32, (block, experts), 0) + b * block
        into = slot - cap * lax.broadcasted_iota(jnp.int32, (block, experts), 1)
        inside = (into >= 0) & (into < cap)
        rank = jnp.sum(jnp.where(inside, into + 1, 0).astype(F32), axis=1, keepdims=True)
        spread = jnp.dot(jnp.where(inside, 1.0, 0.0).astype(BF16), place, preferred_element_type=F32)
        pick = jnp.where(spread == rank, 1.0, 0.0).astype(BF16)
        out = jnp.dot(pick, normed[...], preferred_element_type=F32)
        for k in range(per):
            xs[b * per + k] = out[k * cap : (k + 1) * cap].astype(BF16)
    xr[experts - 1] = xs[fs]

    each_peer(
        lambda m, peer, theirs: remote(
            xs.at[peer], xr.at[theirs], t_send.at[0], t_recv.at[theirs // per], {"fs": peer}
        ).start()
    )

    e1 = lax.broadcasted_iota(jnp.int32, (rows, experts), 1)
    named0 = ids_ref[:, 0:1] == e1
    named1 = ids_ref[:, 1:2] == e1
    after = lax.broadcasted_iota(jnp.int32, (rows, rows), 0) >= lax.broadcasted_iota(jnp.int32, (rows, rows), 1)
    count_t = jnp.dot(
        jnp.where(after, 1.0, 0.0).astype(BF16),
        jnp.where(named0 | named1, 1.0, 0.0).astype(BF16),
        preferred_element_type=F32,
    )
    slot = lax.broadcasted_iota(jnp.int32, (experts, experts * cap), 1)
    into = slot - cap * lax.broadcasted_iota(jnp.int32, (experts, experts * cap), 0)
    inside = (into >= 0) & (into < cap)
    rank = jnp.sum(jnp.where(inside, into + 1, 0).astype(F32), axis=0, keepdims=True)
    fan = jnp.where(inside, 1.0, 0.0).astype(BF16)
    for k, named_k in enumerate((named0, named1)):
        place_k = jnp.where(named_k, count_t, 0.0).astype(BF16)
        spread = jnp.dot(place_k, fan, preferred_element_type=F32)
        sel[k] = jnp.where(spread == rank, 1.0, 0.0).astype(BF16)

    def forward(phase, q):
        for j in range(1, tps):
            dest = xpeer(j)
            remote(
                gu.at[q, pl.ds(dest * span, span)],
                gc.at[q, j - 1],
                g_send.at[phase, j - 1],
                g_recv.at[phase, j - 1],
                {"tp": dest},
            ).start()

    got(gu.at[side, pl.ds(0, experts - 1)], w_sem.at[1])
    y_gu = remote(gu.at[side], gu.at[side], y_send.at[0], y_recv.at[0], {"grp": partner})
    y_gu.start()
    forward(0, side)
    got(dr.at[pl.ds(0, experts - 1), :, my_cols], d_sem.at[1])
    y_down = remote(dr.at[:, :, my_cols], dr.at[:, :, my_cols], y_send.at[1], y_recv.at[1], {"grp": partner})
    y_down.start()
    y_gu.wait_recv()
    forward(1, 1 - side)
    gate_out = pltpu.make_async_copy(gu.at[0], gate_o, o_sem.at[0])
    up_out = pltpu.make_async_copy(gu.at[1], up_o, o_sem.at[1])
    gate_out.start()
    up_out.start()
    y_down.wait_recv()
    out_cols = pl.ds(pl.multiple_of(x * width, width), width)

    def down_send(j):
        dest = xpeer(j)
        return remote(
            dr.at[pl.ds(dest * span, span)],
            down_o.at[:, :, out_cols],
            od_send.at[j - 1],
            od_recv.at[j - 1],
            {"tp": dest},
        )

    for j in range(1, tps):
        down_send(j).start()
    down_own = pltpu.make_async_copy(dr.at[pl.ds(x * span, span)], down_o.at[:, :, out_cols], o_sem.at[2])
    down_own.start()
    for phase, q in ((0, side), (1, 1 - side)):
        for j in range(1, tps):
            remote(
                gc.at[q, j - 1], gc.at[q, j - 1], g_send.at[phase, j - 1], g_recv.at[phase, j - 1], {"tp": xpeer(j)}
            ).wait_recv()

    def weights_for(i):
        parts = []
        for q in range(2):
            w = gu[q, pl.ds(x * span, span)] if i == 0 else gc[q, tps - i - 1]
            parts.append(w.reshape(-1, w.shape[-1]))
        return jnp.concatenate(parts, axis=1)

    def part_send(ch, i):
        return remote(
            ps.at[ch, i - 1], pr.at[ch, i - 1], p_send.at[ch, i - 1], p_recv.at[ch, i - 1], {"tp": xpeer(i)}
        )

    def hid_send(ch, i):
        return remote(hr.at[ch, x], hr.at[ch, x], h_send.at[ch, i - 1], h_recv.at[ch, i - 1], {"tp": xpeer(i)})

    order = [2, 1, 3, 0] if tps == 4 else list(range(1, tps)) + [0]

    def chunk(ch, _):
        @pl.when(ch < CHUNKS - 1)
        def _():
            got(xr.at[pl.ds(ch * per, per)], t_recv.at[ch])

        @pl.when(ch == CHUNKS - 1)
        def _():
            got(xr.at[pl.ds(ch * per, per - 1)], t_recv.at[ch])

        for k in range(per // 2):
            two = [xr[ch * per + 2 * k + i].astype(F32) for i in range(2)]
            x2[2 * k * cap : (2 * k + 2) * cap] = jnp.concatenate(two, axis=0).astype(BF16)
        waiting = None
        for i in order:
            part = jnp.dot(x2[...], weights_for(i), preferred_element_type=F32)
            if i:
                ps[ch, i - 1] = part
            else:
                po[...] = part
            if waiting is not None:
                part_send(ch, waiting).start()
            waiting = i
        for i in range(1, tps):
            part_send(ch, i).wait_recv()
        total = po[...]
        for i in range(1, tps):
            total = total + pr[ch, i - 1]
        ff = total.shape[1] // 2
        gate, up = total[:, :ff], total[:, ff:]
        hr[ch, x] = (gate / (1.0 + jnp.exp(-gate)) * up).astype(BF16)
        for i in range(1, tps):
            hid_send(ch, i).start()
        for i in range(1, tps):
            hid_send(ch, i).wait_recv()
        hidden = jnp.concatenate([hr[ch, i] for i in range(tps)], axis=1)
        out = jnp.dot(hidden, dr[...].reshape(-1, width), preferred_element_type=F32)
        for k in range(per):
            rs[ch * per + k] = out[k * cap : (k + 1) * cap].astype(BF16)

        def back(m, _):
            peer, _theirs = peer_of(m, fs, half)
            remote(rs.at[m], rt.at[fs], r_sem.at[0], r_sem.at[1], {"fs": peer}).start()
            return 0

        lax.fori_loop(ch * per, jnp.minimum(ch * per + per, experts - 1), back, 0)
        return 0

    lax.fori_loop(0, CHUNKS, chunk, 0)
    rt[fs] = rs[experts - 1]

    got(rt.at[pl.ds(0, experts - 1)], r_sem.at[1])

    def flat(i, _):
        two = [rt[2 * i + k].astype(F32) for k in range(2)]
        at = pl.ds(pl.multiple_of(2 * i * cap, 2 * cap), 2 * cap)
        rt2[at] = jnp.concatenate(two, axis=0).astype(BF16)
        return 0

    lax.fori_loop(0, experts // 2, flat, 0)
    mixed = jnp.dot(sel[0], rt2[...], preferred_element_type=F32) * wts_ref[:, 0:1]
    mixed = mixed + jnp.dot(sel[1], rt2[...], preferred_element_type=F32) * wts_ref[:, 1:2]
    mixed_v[...] = mixed.astype(BF16)
    mixed_out = pltpu.make_async_copy(mixed_v, mixed_o, o_sem.at[3])
    mixed_out.start()

    sent(ws.at[pl.ds(0, experts - 1)], w_sem.at[0])
    sent(ds.at[pl.ds(0, experts - 1)], d_sem.at[0])
    sent(xs.at[pl.ds(0, experts - 1)], t_send.at[0])
    sent(rs.at[pl.ds(0, experts - 1)], r_sem.at[0])
    y_gu.wait_send()
    y_down.wait_send()
    y_down_j = range(1, tps)
    for j in y_down_j:
        remote(sq.at[0], sq.at[j], sq_send.at[j - 1], sq_recv.at[j - 1], {"tp": xpeer(j)}).wait_send()
        down_send(j).wait()
        for phase in range(2):
            remote(
                gc.at[0, 0], gc.at[0, 0], g_send.at[phase, j - 1], g_recv.at[phase, j - 1], {"tp": xpeer(j)}
            ).wait_send()
        for ch in range(CHUNKS):
            part_send(ch, j).wait_send()
            hid_send(ch, j).wait_send()
    gate_out.wait()
    up_out.wait()
    down_own.wait()
    mixed_out.wait()


def shards(tps, experts, tokens, norm_gain, gate_master, up_master, down_master, expert_ids, route_weights):
    rows, width = tokens.shape
    top = expert_ids.shape[1]
    cap = top * rows // experts
    _, depth, ff = gate_master.shape
    hid = down_master.shape[1]
    span = experts // tps
    block = experts // CHUNKS * cap
    gain = jnp.broadcast_to(norm_gain[:, None], (depth, ff))
    dma = pltpu.SemaphoreType.DMA
    vmem = pltpu.VMEM
    spec_v = pl.BlockSpec(memory_space=pltpu.VMEM)
    spec_a = pl.BlockSpec(memory_space=pl.ANY)
    gate, up, down, mixed = pl.pallas_call(
        functools.partial(kernel, (experts, tps, rows, top, cap)),
        out_shape=(
            jax.ShapeDtypeStruct((experts, depth, ff), BF16),
            jax.ShapeDtypeStruct((experts, depth, ff), BF16),
            jax.ShapeDtypeStruct((span, hid, width * tps), BF16),
            jax.ShapeDtypeStruct((rows, width), BF16),
        ),
        in_specs=[spec_a, spec_v, spec_a, spec_a, spec_a, spec_v, spec_v, spec_v],
        out_specs=[spec_a] * 4,
        scratch_shapes=[
            vmem((rows, width), BF16),
            vmem((experts, depth, ff), F32),
            vmem((experts, hid, width // 2), F32),
            vmem((experts, depth, ff), BF16),
            vmem((experts, hid, width // 2), BF16),
            vmem((2, experts, depth, ff), BF16),
            vmem((2, tps - 1, span, depth, ff), BF16),
            vmem((experts, hid, width), BF16),
            vmem((rows, width), BF16),
            vmem((experts, cap, width), BF16),
            vmem((experts, cap, width), BF16),
            vmem((block, width), BF16),
            vmem((CHUNKS, tps - 1, block, 2 * ff), F32),
            vmem((CHUNKS, tps - 1, block, 2 * ff), F32),
            vmem((block, 2 * ff), F32),
            vmem((CHUNKS, tps, block, ff), BF16),
            vmem((experts, cap, width), BF16),
            vmem((experts, cap, width), BF16),
            vmem((experts * cap, width), BF16),
            vmem((top, rows, experts * cap), BF16),
            vmem((tps, rows, 128), F32),
            vmem((rows, width), BF16),
            dma((3,)),
            dma((2,)),
            dma((2,)),
            dma((2,)),
            dma((2,)),
            dma((2, tps - 1)),
            dma((2, tps - 1)),
            dma((tps - 1,)),
            dma((tps - 1,)),
            dma((1,)),
            dma((CHUNKS,)),
            dma((CHUNKS, tps - 1)),
            dma((CHUNKS, tps - 1)),
            dma((CHUNKS, tps - 1)),
            dma((CHUNKS, tps - 1)),
            dma((2,)),
            dma((4,)),
            dma((tps - 1,)),
            dma((tps - 1,)),
        ],
        compiler_params=pltpu.CompilerParams(
            collective_id=0, has_side_effects=True, vmem_limit_bytes=60 * 1024 * 1024
        ),
    )(tokens, gain, gate_master, up_master, down_master, expert_ids, expert_ids.T, route_weights)
    return (
        gate.reshape(1, experts * depth, ff),
        up.reshape(1, experts * depth, ff),
        down.reshape(1, span * hid, width * tps),
        mixed,
    )


def solution(mesh):
    return jax.shard_map(
        functools.partial(shards, mesh.shape["tp"], mesh.shape["fs"]),
        mesh=mesh,
        in_specs=(
            P(("grp", "fs"), "tp"),
            P("fs"),
            P(None, "fs", "tp"),
            P(None, "fs", "tp"),
            P(None, "fs", "tp"),
            P(("grp", "fs"), None),
            P(("grp", "fs"), None),
        ),
        out_specs=(
            P(("grp", "fs"), None, "tp"),
            P(("grp", "fs"), None, "tp"),
            P(("grp", "fs"), "tp", None),
            P(("grp", "fs"), "tp"),
        ),
        check_vma=False,
    )
```

time: 512 us -> 244 us (0.48)
  waiting for transfers between devices: 289 us -> 0 us
  Pallas kernels: 0 us -> 234 us
  blocking collectives: 80.5 us -> 0 us
  starting transfers between devices: 51.3 us -> 0 us
  other arithmetic: 26.6 us -> 0 us
  local copies, waits for them, and re-layouts: 29.7 us -> 9.61 us
  matrix products: 17.3 us -> 0 us
  between operations: 14.4 us -> 0.66 us
    all_to_all x6 -> x0, waiting for transfers between devices: 288 us -> none  [the longest x1 98.2 us: sent_together(): lax.all_to_all(both, axis, split_axis=split_dim, concat_axis=concat_dim,...]
    pallas_call x0 -> x1, Pallas kernels: none -> 234 us  [shards(): pl.pallas_call(functools.partial(kernel, (experts, tps, rows, top, cap)),...]
    all_to_all x2 -> x0, blocking collectives: 80.5 us -> none  [the longest x1 73.3 us: shards(): lax.all_to_all(split_blocks, 'tp', split_axis=1, concat_axis=1, tiled=True)]
    all_to_all x6 -> x0, starting transfers between devices: 51.2 us -> none  [the longest x1 26.1 us: shards(): lax.all_to_all(down_master.astype(jnp.bfloat16), FS, split_axis=0, concat...]
    dot_general x2 -> x0, matrix products: 17.3 us -> none  [the longest x1 12 us: shards(): jnp.dot(hidden, down_local[0], preferred_element_type=jnp.float32)]
    reduce_sum x5 -> x0, other arithmetic: 11.2 us -> none  [the longest x1 4.91 us: shards(): summed = jnp.sum(received.astype(jnp.float32), axis=1).astype(jnp.bfloat16)]
    gather x2 -> x0, local copies, waits for them, and re-layouts: 7.14 us -> none  [the longest x1 3.58 us: shards(): outbound = normed[owners].reshape(experts, capacity, tokens.shape[1])]
    unnamed x1 -> x0, other arithmetic: 6.78 us -> none
  transfers between devices with their start and end apart: 7 -> 0, of which waited for: 6 -> 0; matrix products, arithmetic and copies ran while one was open for 6% -> 0% of each run, Pallas kernels for 0% -> 0%
where the time goes in v1:
time: 244 us
  Pallas kernels  234 us (96%)
  local copies, waits for them, and re-layouts  9.61 us (4%)
    pallas_call x1, Pallas kernels, shards(): pl.pallas_call(functools.partial(kernel, (experts, tps, rows, top, cap)),...  234 us
    unnamed x12, local copies, waits for them, and re-layouts  8.24 us

profile of v1, /device:TPU:33, one launch (start us, length us, event | category | flops | bytes accessed | tf_op | source)
XLA Modules:
  0.0 244.2 jit_solution(18064688664205281247)
XLA Ops:
  0.6 1.4 broadcast_in_dim.2.gain_ref
  2.0 1.5 copy.12.wts_ref
  3.5 1.5 copy.11.ids_ref
  5.0 234.0 %shard_map.102 = (bf16[32,128,128]{2,1,0:T(8,128)(2,1)}, bf16[32,128,128]{2,1,0:T(8,128)(2,1)}, bf16[8,16,4096]{2,1,0:T(8,128)(2,1)}, bf16[384,1024]{1,0:T(8,128)(2,1)}) custom-call(bf16[384,1024]{1,0:T(8,128)(2,1)} %tok_h.1, f32[128,128]{1,0:T(8,128)} %broadcast_in_dim.2.gain_ref, f32[32,128,128]{2,1,0:T(8,128)} %gate_h.1, f32[32,128,128]{2,1,0:T(8,128)} %up_h.1, ...), custom_call_target="tpu_custom_call" | custom-call | tf_op jit(solution)/shard_map/pallas_call | solution.py:352
  239.0 0.0 copy-start.1
  239.0 0.0 copy-start
  239.0 2.4 copy.17
  241.4 0.0 copy-done.1
  241.4 0.0 copy-start.2
  241.4 1.0 copy.18
  242.4 0.0 copy-done
  242.4 1.0 copy.19
  243.4 0.0 copy-done.2
  243.4 0.9 copy.20
Async XLA Ops:
  239.0 2.4 copy-start.1
  239.0 3.4 %copy-start = (bf16[8,16,4096]{2,1,0:T(8,128)(2,1)S(1)}, bf16[8,16,4096]{2,1,0:T(8,128)(2,1)}, u32[]{:S(2)}) copy-start(bf16[8,16,4096]{2,1,0:T(8,128)(2,1)} %get-tuple-element.10) | copy-start | bytes 3145732
  241.4 1.9 copy-start.2

commit v2 on v1

--- a/solution.py
+++ b/solution.py
@@ -27,9 +27,9 @@
 
 def kernel(
     sizes,
-    tok_h, gain_ref, gate_h, up_h, down_h, ids_ref, idst_ref, wts_ref,
-    gate_o, up_o, down_o, mixed_o,
-    tok, wf, df, ws, ds, gu, gc, dr, normed, xs, xr, x2, ps, pr, po, hr, rs, rt, rt2, sel, sq, mixed_v,
+    tok_h, gain_ref, gate_h, up_h, down_h, idst_ref, wtst_ref,
+    gate_o, up_o, down_o, rt, sel_o, wts_o,
+    tok, wf, df, ws, ds, gu, gc, dr, normed, xs, xr, x2, ps, pr, po, hr, rs, sel, wts, sq,
     load_sem, w_sem, d_sem, y_send, y_recv, g_send, g_recv, sq_send, sq_recv, t_send, t_recv,
     p_send, p_recv, h_send, h_recv, r_sem, o_sem, od_send, od_recv,
 ):
@@ -92,10 +92,12 @@
         pl.semaphore_signal(barrier, inc=1, device_id={"tp": xpeer(j)}, device_id_type=MESH)
     pl.semaphore_signal(barrier, inc=1, device_id={"grp": partner}, device_id_type=MESH)
 
+    depth, ff = wf.shape[1], wf.shape[2]
+    gain = jnp.broadcast_to(gain_ref[0:1, :], (depth, depth)).T[:, 0:1]
     pltpu.make_async_copy(gate_h, wf, load_sem.at[1]).wait()
 
     def cast_w(e, _):
-        ws[e] = (gain_ref[...] * wf[e]).astype(BF16)
+        ws[e] = (gain * wf[e]).astype(BF16)
         return 0
 
     lax.fori_loop(0, experts, cast_w, 0)
@@ -165,9 +167,14 @@
         ).start()
     )
 
-    e1 = lax.broadcasted_iota(jnp.int32, (rows, experts), 1)
-    named0 = ids_ref[:, 0:1] == e1
-    named1 = ids_ref[:, 1:2] == e1
+    line = lax.broadcasted_iota(jnp.int32, (128, rows), 0)
+    turned = jnp.where(line == 0, idst_ref[0:1, :].astype(F32), idst_ref[1:2, :].astype(F32))
+    turned = jnp.where(line == 2, wtst_ref[0:1, :], turned)
+    turned = jnp.where(line == 3, wtst_ref[1:2, :], turned).T
+    wts[...] = turned
+    e1 = lax.broadcasted_iota(jnp.int32, (rows, experts), 1).astype(F32)
+    named0 = turned[:, 0:1] == e1
+    named1 = turned[:, 1:2] == e1
     after = lax.broadcasted_iota(jnp.int32, (rows, rows), 0) >= lax.broadcasted_iota(jnp.int32, (rows, rows), 1)
     count_t = jnp.dot(
         jnp.where(after, 1.0, 0.0).astype(BF16),
@@ -183,6 +190,10 @@
         place_k = jnp.where(named_k, count_t, 0.0).astype(BF16)
         spread = jnp.dot(place_k, fan, preferred_element_type=F32)
         sel[k] = jnp.where(spread == rank, 1.0, 0.0).astype(BF16)
+    sel_out = pltpu.make_async_copy(sel, sel_o, o_sem.at[4])
+    wts_out = pltpu.make_async_copy(wts, wts_o, o_sem.at[5])
+    sel_out.start()
+    wts_out.start()
 
     def forward(phase, q):
         for j in range(1, tps):
@@ -296,22 +307,9 @@
         return 0
 
     lax.fori_loop(0, CHUNKS, chunk, 0)
-    rt[fs] = rs[experts - 1]
-
+    own_back = pltpu.make_async_copy(rs.at[experts - 1], rt.at[fs], o_sem.at[3])
+    own_back.start()
     got(rt.at[pl.ds(0, experts - 1)], r_sem.at[1])
-
-    def flat(i, _):
-        two = [rt[2 * i + k].astype(F32) for k in range(2)]
-        at = pl.ds(pl.multiple_of(2 * i * cap, 2 * cap), 2 * cap)
-        rt2[at] = jnp.concatenate(two, axis=0).astype(BF16)
-        return 0
-
-    lax.fori_loop(0, experts // 2, flat, 0)
-    mixed = jnp.dot(sel[0], rt2[...], preferred_element_type=F32) * wts_ref[:, 0:1]
-    mixed = mixed + jnp.dot(sel[1], rt2[...], preferred_element_type=F32) * wts_ref[:, 1:2]
-    mixed_v[...] = mixed.astype(BF16)
-    mixed_out = pltpu.make_async_copy(mixed_v, mixed_o, o_sem.at[3])
-    mixed_out.start()
 
     sent(ws.at[pl.ds(0, experts - 1)], w_sem.at[0])
     sent(ds.at[pl.ds(0, experts - 1)], d_sem.at[0])
@@ -319,8 +317,7 @@
     sent(rs.at[pl.ds(0, experts - 1)], r_sem.at[0])
     y_gu.wait_send()
     y_down.wait_send()
-    y_down_j = range(1, tps)
-    for j in y_down_j:
+    for j in range(1, tps):
         remote(sq.at[0], sq.at[j], sq_send.at[j - 1], sq_recv.at[j - 1], {"tp": xpeer(j)}).wait_send()
         down_send(j).wait()
         for phase in range(2):
@@ -333,7 +330,52 @@
     gate_out.wait()
     up_out.wait()
     down_own.wait()
-    mixed_out.wait()
+    own_back.wait()
+    sel_out.wait()
+    wts_out.wait()
+
+
+def finish(
+    gate_h, up_h, down_h, rt_h, sel_h, wts_h,
+    gate_o, up_o, down_o, mixed_o,
+    gate, up, down, rt, sel, wts, flat, mixed, in_sem, out_sem,
+):
+    experts, cap, _width = rt.shape
+    loads = [
+        pltpu.make_async_copy(src, dst, in_sem.at[k])
+        for k, (src, dst) in enumerate(
+            ((rt_h, rt), (sel_h, sel), (wts_h, wts), (gate_h, gate), (up_h, up), (down_h, down))
+        )
+    ]
+    for load in loads:
+        load.start()
+    loads[0].wait()
+
+    def pair(i, _):
+        two = [rt[2 * i + k].astype(F32) for k in range(2)]
+        at = pl.ds(pl.multiple_of(2 * i * cap, 2 * cap), 2 * cap)
+        flat[at] = jnp.concatenate(two, axis=0).astype(BF16)
+        return 0
+
+    lax.fori_loop(0, experts // 2, pair, 0)
+    loads[1].wait()
+    loads[2].wait()
+    stores = []
+    for k, (src, dst) in enumerate(((gate, gate_o), (up, up_o), (down, down_o))):
+        loads[3 + k].wait()
+        stores.append(pltpu.make_async_copy(src, dst, out_sem.at[k]))
+        stores[-1].start()
+    parts = 2
+    size = mixed.shape[0] // parts
+    for p in range(parts):
+        at = pl.ds(p * size, size)
+        out = jnp.dot(sel[0, at], flat[...], preferred_element_type=F32) * wts[at, 2:3]
+        out = out + jnp.dot(sel[1, at], flat[...], preferred_element_type=F32) * wts[at, 3:4]
+        mixed[at] = out.astype(BF16)
+        stores.append(pltpu.make_async_copy(mixed.at[at], mixed_o.at[at], out_sem.at[3 + p]))
+        stores[-1].start()
+    for store in stores:
+        store.wait()
 
 
 def shards(tps, experts, tokens, norm_gain, gate_master, up_master, down_master, expert_ids, route_weights):
@@ -344,21 +386,22 @@
     hid = down_master.shape[1]
     span = experts // tps
     block = experts // CHUNKS * cap
-    gain = jnp.broadcast_to(norm_gain[:, None], (depth, ff))
     dma = pltpu.SemaphoreType.DMA
     vmem = pltpu.VMEM
     spec_v = pl.BlockSpec(memory_space=pltpu.VMEM)
     spec_a = pl.BlockSpec(memory_space=pl.ANY)
-    gate, up, down, mixed = pl.pallas_call(
+    moved = pl.pallas_call(
         functools.partial(kernel, (experts, tps, rows, top, cap)),
         out_shape=(
             jax.ShapeDtypeStruct((experts, depth, ff), BF16),
             jax.ShapeDtypeStruct((experts, depth, ff), BF16),
             jax.ShapeDtypeStruct((span, hid, width * tps), BF16),
-            jax.ShapeDtypeStruct((rows, width), BF16),
+            jax.ShapeDtypeStruct((experts, cap, width), BF16),
+            jax.ShapeDtypeStruct((top, rows, experts * cap), BF16),
+            jax.ShapeDtypeStruct((rows, 128), F32),
         ),
-        in_specs=[spec_a, spec_v, spec_a, spec_a, spec_a, spec_v, spec_v, spec_v],
-        out_specs=[spec_a] * 4,
+        in_specs=[spec_a, spec_v, spec_a, spec_a, spec_a, spec_v, spec_v],
+        out_specs=[spec_a] * 6,
         scratch_shapes=[
             vmem((rows, width), BF16),
             vmem((experts, depth, ff), F32),
@@ -377,11 +420,9 @@
             vmem((block, 2 * ff), F32),
             vmem((CHUNKS, tps, block, ff), BF16),
             vmem((experts, cap, width), BF16),
-            vmem((experts, cap, width), BF16),
-            vmem((experts * cap, width), BF16),
             vmem((top, rows, experts * cap), BF16),
+            vmem((rows, 128), F32),
             vmem((tps, rows, 128), F32),
-            vmem((rows, width), BF16),
             dma((3,)),
             dma((2,)),
             dma((2,)),
@@ -398,14 +439,33 @@
             dma((CHUNKS, tps - 1)),
             dma((CHUNKS, tps - 1)),
             dma((2,)),
-            dma((4,)),
+            dma((6,)),
             dma((tps - 1,)),
             dma((tps - 1,)),
         ],
         compiler_params=pltpu.CompilerParams(
             collective_id=0, has_side_effects=True, vmem_limit_bytes=60 * 1024 * 1024
         ),
-    )(tokens, gain, gate_master, up_master, down_master, expert_ids, expert_ids.T, route_weights)
+    )(tokens, norm_gain.reshape(1, depth), gate_master, up_master, down_master, expert_ids.T, route_weights.T)
+    shapes = [m.shape for m in moved]
+    gate, up, down, mixed = pl.pallas_call(
+        finish,
+        out_shape=(
+            *(jax.ShapeDtypeStruct(shape, BF16) for shape in shapes[:3]),
+            jax.ShapeDtypeStruct((rows, width), BF16),
+        ),
+        in_specs=[spec_a] * 6,
+        out_specs=[spec_a] * 4,
+        scratch_shapes=[
+            *(vmem(shape, BF16) for shape in shapes[:5]),
+            vmem(shapes[5], F32),
+            vmem((experts * cap, width), BF16),
+            vmem((rows, width), BF16),
+            dma((6,)),
+            dma((5,)),
+        ],
+        compiler_params=pltpu.CompilerParams(vmem_limit_bytes=60 * 1024 * 1024),
+    )(*moved)
     return (
         gate.reshape(1, experts * depth, ff),
         up.reshape(1, experts * depth, ff),

time: 244 us -> 238 us (0.975)
  local copies, waits for them, and re-layouts: 9.61 us -> 0 us
  Pallas kernels: 234 us -> 237 us
    unnamed x12 -> x0, local copies, waits for them, and re-layouts: 8.24 us -> none
    pallas_call x0 -> x1, Pallas kernels: none -> 5.01 us  [shards(): pl.pallas_call(finish, out_shape=(*(jax.ShapeDtypeStruct(shape, BF16) for...]
where the time goes in v2:
time: 238 us
  Pallas kernels  237 us (100%)
    pallas_call x1, Pallas kernels, shards(): pl.pallas_call(functools.partial(kernel, (experts, tps, rows, top, cap)),...  232 us
    pallas_call x1, Pallas kernels, shards(): pl.pallas_call(finish, out_shape=(*(jax.ShapeDtypeStruct(shape, BF16) for...  5.01 us

profile of v2, /device:TPU:33, one launch (start us, length us, event | category | flops | bytes accessed | tf_op | source)
XLA Modules:
  0.0 237.7 jit_solution(6446933974028264386)
XLA Ops:
  0.6 232.0 %shard_map.102 = (bf16[32,128,128]{2,1,0:T(8,128)(2,1)}, bf16[32,128,128]{2,1,0:T(8,128)(2,1)}, bf16[8,16,4096]{2,1,0:T(8,128)(2,1)}, bf16[32,24,1024]{2,1,0:T(8...) custom-call(bf16[384,1024]{1,0:T(8,128)(2,1)} %tok_h.1, f32[1,128]{1,0:T(1,128)} %bitcast.8, ...), custom_call_target="tpu_custom_call" | custom-call | tf_op jit(solution)/shard_map/pallas_call | solution.py:393
  232.7 5.0 %shard_map.103 = (bf16[32,128,128]{2,1,0:T(8,128)(2,1)}, bf16[32,128,128]{2,1,0:T(8,128)(2,1)}, bf16[8,16,4096]{2,1,0:T(8,128)(2,1)}, bf16[384,1024]{1,0:T(8,128)(2,1)}) custom-call(bf16[32,128,128]{2,1,0:T(8,128)(2,1)} %get-tuple-element.14.gate_h, bf16[32,128,128]{2,1,0:T(8,128)(2,1)} %get-tuple-element.15.up_h, ...), custom_call_target="tpu_custom_call" | custom-call | tf_op jit(solution)/shard_map/pallas_call | solution.py:451

commit v3 on v2

--- a/solution.py
+++ b/solution.py
@@ -31,7 +31,7 @@
     gate_o, up_o, down_o, rt, sel_o, wts_o,
     tok, wf, df, ws, ds, gu, gc, dr, normed, xs, xr, x2, ps, pr, po, hr, rs, sel, wts, sq,
     load_sem, w_sem, d_sem, y_send, y_recv, g_send, g_recv, sq_send, sq_recv, t_send, t_recv,
-    p_send, p_recv, h_send, h_recv, r_sem, o_sem, od_send, od_recv,
+    p_send, p_recv, h_send, h_recv, r_sem, o_sem, od_send, od_recv, low_sem, high_sem,
 ):
     experts, tps, rows, top, cap = sizes
     half = experts // 4
@@ -83,11 +83,26 @@
     tok_load.start()
 
     barrier = pltpu.get_barrier_semaphore()
-    each_peer(
-        lambda m, peer, theirs: pl.semaphore_signal(
-            barrier, inc=1, device_id={"fs": peer}, device_id_type=MESH
-        )
-    )
+    rings = 2 * half
+    z, core = fs // 2, fs % 2
+    other = 2 * z + 1 - core
+    has_low, has_high = (z + rings - 1) // rings, 1 - z // (rings - 1)
+
+    def tell(sem, peer):
+        pl.semaphore_signal(sem, inc=1, device_id={"fs": peer}, device_id_type=MESH)
+
+    tell(barrier, other)
+
+    @pl.when(has_low == 1)
+    def _():
+        for c in range(2):
+            tell(barrier, 2 * (z - 1) + c)
+
+    @pl.when(has_high == 1)
+    def _():
+        for c in range(2):
+            tell(barrier, 2 * (z + 1) + c)
+
     for j in range(1, tps):
         pl.semaphore_signal(barrier, inc=1, device_id={"tp": xpeer(j)}, device_id_type=MESH)
     pl.semaphore_signal(barrier, inc=1, device_id={"grp": partner}, device_id_type=MESH)
@@ -102,13 +117,32 @@
 
     lax.fori_loop(0, experts, cast_w, 0)
     gu[side, fs] = ws[fs]
-    pl.semaphore_wait(barrier, experts - 1 + tps - 1 + 1)
-
-    each_peer(
-        lambda m, peer, theirs: remote(
-            ws.at[peer], gu.at[side, fs], w_sem.at[0], w_sem.at[1], {"fs": peer}
-        ).start()
-    )
+    pl.semaphore_wait(barrier, 1 + tps - 1 + 1 + 2 * has_low + 2 * has_high)
+
+    @pl.when(has_low * has_high == 1)
+    def _():
+        tell(low_sem.at[2], fs + 2)
+        tell(high_sem.at[2], fs - 2)
+
+    def w_send(peer):
+        remote(ws.at[peer], gu.at[side, fs], w_sem.at[0], w_sem.at[1], {"fs": peer}).start()
+
+    w_send(other)
+
+    def downward(k, _):
+        @pl.when(k > 1)
+        def _():
+            pl.semaphore_wait(low_sem.at[k], 1)
+
+            @pl.when(has_high == 1)
+            def _():
+                tell(low_sem.at[k + 1], fs + 2)
+
+        for c in range(2):
+            w_send(2 * (z - k) + c)
+        return 0
+
+    lax.fori_loop(1, z + 1, downward, 0)
 
     down_load.wait()
 
@@ -122,13 +156,28 @@
     values = tok[...].astype(F32)
     sq[0] = jnp.broadcast_to(jnp.sum(values * values, axis=1, keepdims=True), sq.shape[1:])
 
+    for j in range(1, tps):
+        remote(sq.at[0], sq.at[j], sq_send.at[j - 1], sq_recv.at[j - 1], {"tp": xpeer(j)}).start()
+
+    def upward(k, _):
+        @pl.when(k > 1)
+        def _():
+            pl.semaphore_wait(high_sem.at[k], 1)
+
+            @pl.when(has_low == 1)
+            def _():
+                tell(high_sem.at[k + 1], fs - 2)
+
+        for c in range(2):
+            w_send(2 * (z + k) + c)
+        return 0
+
+    lax.fori_loop(1, rings - z, upward, 0)
     each_peer(
         lambda m, peer, theirs: remote(
             ds.at[peer], dr.at[fs, :, my_cols], d_sem.at[0], d_sem.at[1], {"fs": peer}
         ).start()
     )
-    for j in range(1, tps):
-        remote(sq.at[0], sq.at[j], sq_send.at[j - 1], sq_recv.at[j - 1], {"tp": xpeer(j)}).start()
 
     block = per * cap
     e0 = lax.broadcasted_iota(jnp.int32, (experts, rows), 0)
@@ -442,6 +491,8 @@
             dma((6,)),
             dma((tps - 1,)),
             dma((tps - 1,)),
+            pltpu.SemaphoreType.REGULAR((experts // 2 + 1,)),
+            pltpu.SemaphoreType.REGULAR((experts // 2 + 1,)),
         ],
         compiler_params=pltpu.CompilerParams(
             collective_id=0, has_side_effects=True, vmem_limit_bytes=60 * 1024 * 1024

time: 238 us -> 244 us (1.025)
  Pallas kernels: 237 us -> 242 us
    pallas_call x1, Pallas kernels: 232 us -> 237 us  [shards(): pl.pallas_call(functools.partial(kernel, (experts, tps, rows, top, cap)),...]
where the time goes in v3:
time: 244 us; the launch traced here: 243 us
  Pallas kernels  242 us (99%)
    pallas_call x1, Pallas kernels, shards(): pl.pallas_call(functools.partial(kernel, (experts, tps, rows, top, cap)),...  237 us
    pallas_call x1, Pallas kernels, shards(): pl.pallas_call(finish, out_shape=(*(jax.ShapeDtypeStruct(shape, BF16) for...  5.01 us

profile of v3, /device:TPU:33, one launch (start us, length us, event | category | flops | bytes accessed | tf_op | source)
XLA Modules:
  0.0 242.9 jit_solution(2045940046253839329)
XLA Ops:
  0.6 237.3 %shard_map.102 = (bf16[32,128,128]{2,1,0:T(8,128)(2,1)}, bf16[32,128,128]{2,1,0:T(8,128)(2,1)}, bf16[8,16,4096]{2,1,0:T(8,128)(2,1)}, bf16[32,24,1024]{2,1,0:T(8...) custom-call(bf16[384,1024]{1,0:T(8,128)(2,1)} %tok_h.1, f32[1,128]{1,0:T(1,128)} %bitcast.8, ...), custom_call_target="tpu_custom_call" | custom-call | tf_op jit(solution)/shard_map/pallas_call | solution.py:442
  237.9 5.0 %shard_map.103 = (bf16[32,128,128]{2,1,0:T(8,128)(2,1)}, bf16[32,128,128]{2,1,0:T(8,128)(2,1)}, bf16[8,16,4096]{2,1,0:T(8,128)(2,1)}, bf16[384,1024]{1,0:T(8,128)(2,1)}) custom-call(bf16[32,128,128]{2,1,0:T(8,128)(2,1)} %get-tuple-element.14.gate_h, bf16[32,128,128]{2,1,0:T(8,128)(2,1)} %get-tuple-element.15.up_h, ...), custom_call_target="tpu_custom_call" | custom-call | tf_op jit(solution)/shard_map/pallas_call | solution.py:502

commit v4 on v2

--- a/solution.py
+++ b/solution.py
@@ -11,6 +11,7 @@
 F32 = jnp.float32
 BF16 = jnp.bfloat16
 CHUNKS = 4
+GROUP = 8
 
 
 def peer_of(m, fs, half):
@@ -25,19 +26,73 @@
     return peer, 2 * (n + sign * inner) + m % 2
 
 
+def classes(shape, axis, home, groups):
+    k = lax.broadcasted_iota(jnp.int32, shape, axis)
+    far = jnp.where(k == GROUP, (home + 1) % groups, jnp.where(k == GROUP + 1, (home + 3) % groups, (home + 2) % groups))
+    low = jnp.where(k < GROUP, GROUP * home + k, GROUP * far)
+    return k, low.astype(F32), (low + jnp.where(k < GROUP, 1, GROUP)).astype(F32)
+
+
+def layout(shape, axis, base, cap, many):
+    row = lax.broadcasted_iota(jnp.int32, shape, 1 - axis) + base
+    k = lax.broadcasted_iota(jnp.int32, shape, axis)
+    into = row - jnp.where(k < GROUP, cap * k, GROUP * cap + many * (k - GROUP))
+    inside = (into >= 0) & (into < jnp.where(k < GROUP, cap, many))
+    number = jnp.sum(jnp.where(inside, into + 1, 0).astype(F32), axis=axis, keepdims=True)
+    return jnp.where(inside, 1.0, 0.0).astype(BF16), number
+
+
+def one(cond):
+    return jnp.where(cond, 1.0, 0.0).astype(BF16)
+
+
+def places(id0, id1, n_classes, home, groups):
+    t = id0.shape[1]
+    _, low, high = classes((n_classes, t), 0, home, groups)
+    named = ((id0 >= low) & (id0 < high)) | ((id1 >= low) & (id1 < high))
+    before = lax.broadcasted_iota(jnp.int32, (t, t), 0) <= lax.broadcasted_iota(jnp.int32, (t, t), 1)
+    count = jnp.dot(one(named), one(before), preferred_element_type=F32)
+    return jnp.where(named, count, 0.0).astype(BF16)
+
+
+def picks(id0, id1, n_classes, home, groups, n_rows, cap, many):
+    t = id0.shape[0]
+    k, low, high = classes((t, n_classes), 1, home, groups)
+    in0 = (id0 >= low) & (id0 < high)
+    in1 = (id1 >= low) & (id1 < high)
+    after = lax.broadcasted_iota(jnp.int32, (t, t), 0) >= lax.broadcasted_iota(jnp.int32, (t, t), 1)
+    count = jnp.dot(one(after), one(in0 | in1), preferred_element_type=F32)
+    fan, number = layout((n_classes, n_rows), 0, 0, cap, many)
+    out = []
+    for named in (in0, in1 & (k < GROUP)):
+        spread = jnp.dot(jnp.where(named, count, 0.0).astype(BF16), fan, preferred_element_type=F32)
+        out.append(one(spread == number))
+    return out
+
+
 def kernel(
     sizes,
     tok_h, gain_ref, gate_h, up_h, down_h, idst_ref, wtst_ref,
-    gate_o, up_o, down_o, rt, sel_o, wts_o,
-    tok, wf, df, ws, ds, gu, gc, dr, normed, xs, xr, x2, ps, pr, po, hr, rs, sel, wts, sq,
+    gate_o, up_o, down_o, rt_near, rt_far, sel_o, wts_o,
+    tok, wf, df, ws, ds, gu, gc, dr, normed, xs, xg, ids, xr, x2, ps, pr, po, hr, rs, sel, wts, sq,
+    eb, ib, rb, xb, mb,
+    e_send, e_recv, i_send, i_recv, rb_send, xb_recv, mb_send, far_recv,
     load_sem, w_sem, d_sem, y_send, y_recv, g_send, g_recv, sq_send, sq_recv, t_send, t_recv,
     p_send, p_recv, h_send, h_recv, r_sem, o_sem, od_send, od_recv,
 ):
     experts, tps, rows, top, cap = sizes
     half = experts // 4
+    rings = 2 * half
+    groups = experts // GROUP
+    many = GROUP * cap // top
     per = experts // CHUNKS
     span = experts // tps
     fs, x, grp = lax.axis_index("fs"), lax.axis_index("tp"), lax.axis_index("grp")
+    z, core = fs // 2, fs % 2
+    other = 2 * z + 1 - core
+    home, mine = fs // GROUP, fs % GROUP
+    pos = mine // 2
+    is_door = 1 - (pos + 1) // 2 % 2
     side = grp % 2
     partner = grp + 1 - 2 * side
     width = tok.shape[1]
@@ -122,24 +177,12 @@
     values = tok[...].astype(F32)
     sq[0] = jnp.broadcast_to(jnp.sum(values * values, axis=1, keepdims=True), sq.shape[1:])
 
-    each_peer(
-        lambda m, peer, theirs: remote(
-            ds.at[peer], dr.at[fs, :, my_cols], d_sem.at[0], d_sem.at[1], {"fs": peer}
-        ).start()
-    )
     for j in range(1, tps):
         remote(sq.at[0], sq.at[j], sq_send.at[j - 1], sq_recv.at[j - 1], {"tp": xpeer(j)}).start()
 
-    block = per * cap
-    e0 = lax.broadcasted_iota(jnp.int32, (experts, rows), 0)
-    named = (idst_ref[0:1, :] == e0) | (idst_ref[1:2, :] == e0)
-    before = lax.broadcasted_iota(jnp.int32, (rows, rows), 0) <= lax.broadcasted_iota(jnp.int32, (rows, rows), 1)
-    count = jnp.dot(
-        jnp.where(named, 1.0, 0.0).astype(BF16),
-        jnp.where(before, 1.0, 0.0).astype(BF16),
-        preferred_element_type=F32,
-    )
-    place = jnp.where(named, count, 0.0).astype(BF16)
+    id0, id1 = idst_ref[0:1, :].astype(F32), idst_ref[1:2, :].astype(F32)
+    place = places(id0, id1, experts, home, groups)
+    near_rows = GROUP * cap
 
     for j in range(1, tps):
         remote(sq.at[0], sq.at[j], sq_send.at[j - 1], sq_recv.at[j - 1], {"tp": xpeer(j)}).wait_recv()
@@ -149,51 +192,116 @@
     scale = lax.rsqrt(total_sq / (width * tps) + 1e-06)
     normed[...] = (tok[...].astype(F32) * scale).astype(BF16)
 
-    for b in range(CHUNKS):
-        slot = lax.broadcasted_iota(jnp.int32, (block, experts), 0) + b * block
-        into = slot - cap * lax.broadcasted_iota(jnp.int32, (block, experts), 1)
-        inside = (into >= 0) & (into < cap)
-        rank = jnp.sum(jnp.where(inside, into + 1, 0).astype(F32), axis=1, keepdims=True)
-        spread = jnp.dot(jnp.where(inside, 1.0, 0.0).astype(BF16), place, preferred_element_type=F32)
-        pick = jnp.where(spread == rank, 1.0, 0.0).astype(BF16)
-        out = jnp.dot(pick, normed[...], preferred_element_type=F32)
-        for k in range(per):
-            xs[b * per + k] = out[k * cap : (k + 1) * cap].astype(BF16)
-    xr[experts - 1] = xs[fs]
+    line = lax.broadcasted_iota(jnp.int32, (8, rows), 0)
+    meta = jnp.where(line == 0, id0, jnp.where(line == 1, id1, 0.0))
+    meta = jnp.where(line == 2, wtst_ref[0:1, :], jnp.where(line == 3, wtst_ref[1:2, :], meta))
+    for f in range(groups - 1):
+        fan, number = layout((many, experts), 1, near_rows + f * many, cap, many)
+        pick = one(jnp.dot(fan, place, preferred_element_type=F32) == number)
+        xg[f] = jnp.dot(pick, normed[...], preferred_element_type=F32).astype(BF16)
+        ids[f] = jnp.zeros(ids.shape[1:], F32)
+        ids[f, :, 0:many] = lax.dot_general(
+            meta,
+            pick.astype(F32),
+            (((1,), (1,)), ((), ())),
+            precision=lax.Precision.HIGHEST,
+            preferred_element_type=F32,
+        )
+    fan, number = layout((near_rows, experts), 1, 0, cap, many)
+    pick = one(jnp.dot(fan, place, preferred_element_type=F32) == number)
+    out = jnp.dot(pick, normed[...], preferred_element_type=F32)
+    for k in range(GROUP):
+        xs[k] = out[k * cap : (k + 1) * cap].astype(BF16)
+    xr[mine] = xs[mine]
+
+    turn = pos // 2
+    hops = (4 - pos, pos + 1, turn * (8 - pos) + (1 - turn) * (pos + 5))
+    doors = (
+        GROUP * ((home + 1) % groups) + core,
+        GROUP * ((home + 3) % groups) + GROUP - 2 + core,
+        GROUP * ((home + 2) % groups) + (GROUP - 2) * (1 - turn) + core,
+    )
+
+    def to_door(f):
+        at = hops[f] - 1
+        return (
+            remote(ids.at[f], ib.at[at], i_send.at[f], i_recv.at[at], {"fs": doors[f]}),
+            remote(xg.at[f], eb.at[at], e_send.at[f], e_recv.at[at], {"fs": doors[f]}),
+        )
+
+    for f in (2, 0, 1):
+        for copy in to_door(f):
+            copy.start()
 
     each_peer(
         lambda m, peer, theirs: remote(
-            xs.at[peer], xr.at[theirs], t_send.at[0], t_recv.at[theirs // per], {"fs": peer}
+            ds.at[peer], dr.at[fs, :, my_cols], d_sem.at[0], d_sem.at[1], {"fs": peer}
         ).start()
     )
 
+    def near(k, _):
+        j = (mine + k) % GROUP
+        remote(xs.at[j], xr.at[mine], t_send.at[0], t_recv.at[0], {"fs": GROUP * home + j}).start()
+        return 0
+
+    lax.fori_loop(1, GROUP, near, 0)
+
     line = lax.broadcasted_iota(jnp.int32, (128, rows), 0)
-    turned = jnp.where(line == 0, idst_ref[0:1, :].astype(F32), idst_ref[1:2, :].astype(F32))
+    turned = jnp.where(line == 0, id0, id1)
     turned = jnp.where(line == 2, wtst_ref[0:1, :], turned)
     turned = jnp.where(line == 3, wtst_ref[1:2, :], turned).T
-    wts[...] = turned
-    e1 = lax.broadcasted_iota(jnp.int32, (rows, experts), 1).astype(F32)
-    named0 = turned[:, 0:1] == e1
-    named1 = turned[:, 1:2] == e1
-    after = lax.broadcasted_iota(jnp.int32, (rows, rows), 0) >= lax.broadcasted_iota(jnp.int32, (rows, rows), 1)
-    count_t = jnp.dot(
-        jnp.where(after, 1.0, 0.0).astype(BF16),
-        jnp.where(named0 | named1, 1.0, 0.0).astype(BF16),
-        preferred_element_type=F32,
-    )
-    slot = lax.broadcasted_iota(jnp.int32, (experts, experts * cap), 1)
-    into = slot - cap * lax.broadcasted_iota(jnp.int32, (experts, experts * cap), 0)
-    inside = (into >= 0) & (into < cap)
-    rank = jnp.sum(jnp.where(inside, into + 1, 0).astype(F32), axis=0, keepdims=True)
-    fan = jnp.where(inside, 1.0, 0.0).astype(BF16)
-    for k, named_k in enumerate((named0, named1)):
-        place_k = jnp.where(named_k, count_t, 0.0).astype(BF16)
-        spread = jnp.dot(place_k, fan, preferred_element_type=F32)
-        sel[k] = jnp.where(spread == rank, 1.0, 0.0).astype(BF16)
+    lane = lax.broadcasted_iota(jnp.int32, turned.shape, 1)
+    first = turned[:, 0:1]
+    home_low = (GROUP * home).astype(F32)
+    away = (first < home_low) | (first >= home_low + GROUP)
+    wts[...] = jnp.where((lane == 2) & away, 1.0, turned)
+    both = picks(first, turned[:, 1:2], experts, home, groups, near_rows + (groups - 1) * many, cap, many)
+    for k in range(2):
+        sel[k] = both[k]
     sel_out = pltpu.make_async_copy(sel, sel_o, o_sem.at[4])
     wts_out = pltpu.make_async_copy(wts, wts_o, o_sem.at[5])
     sel_out.start()
     wts_out.start()
+
+    def slot_of(i, way, c):
+        return GROUP + (5 - i) * 4 + way * 2 + c
+
+    def hand_on(i):
+        @pl.when(is_door == 1)
+        def _():
+            remote(ids.at[0], ib.at[i], i_send.at[0], i_recv.at[i], {"fs": other}).wait_recv()
+            remote(xg.at[0], eb.at[i], e_send.at[0], e_recv.at[i], {"fs": other}).wait_recv()
+            spots = places(ib[i, 0:1, 0:many], ib[i, 1:2, 0:many], experts, home, groups)
+            fan, number = layout((near_rows, experts), 1, 0, cap, many)
+            pick = one(jnp.dot(fan, spots, preferred_element_type=F32) == number)
+            out = jnp.dot(pick, eb[i], preferred_element_type=F32)
+            for k in range(GROUP):
+                rb[i * GROUP + k] = out[k * cap : (k + 1) * cap].astype(BF16)
+            slot = slot_of(i, turn, core)
+            xr[slot] = rb[i * GROUP + mine]
+
+            def give(k, _):
+                j = (mine + k) % GROUP
+                remote(
+                    rb.at[i * GROUP + j], xr.at[slot], rb_send.at[0], t_recv.at[slot // per], {"fs": GROUP * home + j}
+                ).start()
+                return 0
+
+            lax.fori_loop(1, GROUP, give, 0)
+
+    def hand_back(i):
+        @pl.when(is_door == 1)
+        def _():
+            got(xb.at[pl.ds(0, GROUP - 1)], xb_recv.at[i])
+            turned = jnp.concatenate([ib[i]] * 16, axis=0).T[0:many]
+            two = picks(turned[:, 0:1], turned[:, 1:2], experts, home, groups, near_rows, cap, many)
+            flat = jnp.concatenate([xb[i * GROUP + k].astype(F32) for k in range(GROUP)], axis=0).astype(BF16)
+            out = jnp.dot(two[0], flat, preferred_element_type=F32) * turned[:, 2:3]
+            out = out + jnp.dot(two[1], flat, preferred_element_type=F32) * turned[:, 3:4]
+            mb[i] = out.astype(BF16)
+            f = turn if i < 4 else 2
+            back_to = (z + (2 * turn - 1) * (i + 1) + rings) % rings
+            remote(mb.at[i], rt_far.at[f], mb_send.at[0], far_recv.at[f], {"fs": 2 * back_to + core}).start()
 
     def forward(phase, q):
         for j in range(1, tps):
@@ -210,16 +318,12 @@
     y_gu = remote(gu.at[side], gu.at[side], y_send.at[0], y_recv.at[0], {"grp": partner})
     y_gu.start()
     forward(0, side)
-    got(dr.at[pl.ds(0, experts - 1), :, my_cols], d_sem.at[1])
-    y_down = remote(dr.at[:, :, my_cols], dr.at[:, :, my_cols], y_send.at[1], y_recv.at[1], {"grp": partner})
-    y_down.start()
     y_gu.wait_recv()
     forward(1, 1 - side)
     gate_out = pltpu.make_async_copy(gu.at[0], gate_o, o_sem.at[0])
     up_out = pltpu.make_async_copy(gu.at[1], up_o, o_sem.at[1])
     gate_out.start()
     up_out.start()
-    y_down.wait_recv()
     out_cols = pl.ds(pl.multiple_of(x * width, width), width)
 
     def down_send(j):
@@ -232,10 +336,9 @@
             {"tp": dest},
         )
 
-    for j in range(1, tps):
-        down_send(j).start()
     down_own = pltpu.make_async_copy(dr.at[pl.ds(x * span, span)], down_o.at[:, :, out_cols], o_sem.at[2])
-    down_own.start()
+    for i in range(5, -1, -1):
+        hand_on(i)
     for phase, q in ((0, side), (1, 1 - side)):
         for j in range(1, tps):
             remote(
@@ -257,16 +360,20 @@
     def hid_send(ch, i):
         return remote(hr.at[ch, x], hr.at[ch, x], h_send.at[ch, i - 1], h_recv.at[ch, i - 1], {"tp": xpeer(i)})
 
-    order = [2, 1, 3, 0] if tps == 4 else list(range(1, tps)) + [0]
-
-    def chunk(ch, _):
-        @pl.when(ch < CHUNKS - 1)
-        def _():
-            got(xr.at[pl.ds(ch * per, per)], t_recv.at[ch])
-
-        @pl.when(ch == CHUNKS - 1)
-        def _():
-            got(xr.at[pl.ds(ch * per, per - 1)], t_recv.at[ch])
+    order = [2, 1, 3, 0]
+
+    def contract(ch):
+        if ch == 0:
+            got(xr.at[pl.ds(0, per - 1)], t_recv.at[0])
+        else:
+
+            @pl.when(is_door == 1)
+            def _():
+                got(xr.at[pl.ds(0, per - 2)], t_recv.at[ch])
+
+            @pl.when(is_door == 0)
+            def _():
+                got(xr.at[pl.ds(0, per)], t_recv.at[ch])
 
         for k in range(per // 2):
             two = [xr[ch * per + 2 * k + i].astype(F32) for i in range(2)]
@@ -275,22 +382,26 @@
         for i in order:
             part = jnp.dot(x2[...], weights_for(i), preferred_element_type=F32)
             if i:
-                ps[ch, i - 1] = part
+                ps[ch, i - 1] = part.astype(BF16)
             else:
-                po[...] = part
+                po[ch] = part
             if waiting is not None:
                 part_send(ch, waiting).start()
-            waiting = i
+            waiting = i or None
+
+    def activate(ch):
         for i in range(1, tps):
             part_send(ch, i).wait_recv()
-        total = po[...]
+        total = po[ch]
         for i in range(1, tps):
-            total = total + pr[ch, i - 1]
+            total = total + pr[ch, i - 1].astype(F32)
         ff = total.shape[1] // 2
         gate, up = total[:, :ff], total[:, ff:]
         hr[ch, x] = (gate / (1.0 + jnp.exp(-gate)) * up).astype(BF16)
         for i in range(1, tps):
             hid_send(ch, i).start()
+
+    def project(ch):
         for i in range(1, tps):
             hid_send(ch, i).wait_recv()
         hidden = jnp.concatenate([hr[ch, i] for i in range(tps)], axis=1)
@@ -298,23 +409,77 @@
         for k in range(per):
             rs[ch * per + k] = out[k * cap : (k + 1) * cap].astype(BF16)
 
-        def back(m, _):
-            peer, _theirs = peer_of(m, fs, half)
-            remote(rs.at[m], rt.at[fs], r_sem.at[0], r_sem.at[1], {"fs": peer}).start()
-            return 0
-
-        lax.fori_loop(ch * per, jnp.minimum(ch * per + per, experts - 1), back, 0)
-        return 0
-
-    lax.fori_loop(0, CHUNKS, chunk, 0)
-    own_back = pltpu.make_async_copy(rs.at[experts - 1], rt.at[fs], o_sem.at[3])
+        if ch == 0:
+
+            def back(k, _):
+                j = (mine + k) % GROUP
+                remote(rs.at[j], rt_near.at[mine], r_sem.at[0], r_sem.at[1], {"fs": GROUP * home + j}).start()
+                return 0
+
+            lax.fori_loop(1, GROUP, back, 0)
+        else:
+
+            def back(k, _):
+                i = 5 - (2 * (ch - 1) + k // 4)
+                door = GROUP * home + (GROUP - 2) * (k % 4 // 2) + k % 2
+                spot = i * GROUP + mine
+
+                @pl.when(door == fs)
+                def _():
+                    xb[spot] = rs[ch * per + k]
+
+                @pl.when(door != fs)
+                def _():
+                    remote(rs.at[ch * per + k], xb.at[spot], r_sem.at[0], xb_recv.at[i], {"fs": door}).start()
+
+                return 0
+
+            lax.fori_loop(0, per, back, 0)
+
+    got(dr.at[pl.ds(0, experts - 1), :, my_cols], d_sem.at[1])
+    y_down = remote(dr.at[:, :, my_cols], dr.at[:, :, my_cols], y_send.at[1], y_recv.at[1], {"grp": partner})
+    y_down.start()
+    contract(1)
+    activate(1)
+    y_down.wait_recv()
+    project(1)
+    contract(2)
+    activate(2)
+    contract(0)
+    project(2)
+    contract(3)
+    activate(0)
+    activate(3)
+    project(0)
+    project(3)
+    for j in range(1, tps):
+        down_send(j).start()
+    down_own.start()
+    for i in range(5, -1, -1):
+        hand_back(i)
+    own_back = pltpu.make_async_copy(rs.at[mine], rt_near.at[mine], o_sem.at[3])
     own_back.start()
-    got(rt.at[pl.ds(0, experts - 1)], r_sem.at[1])
+    got(rt_near.at[pl.ds(0, GROUP - 1)], r_sem.at[1])
+    for f in range(groups - 1):
+        got(rt_far.at[f], far_recv.at[f])
 
     sent(ws.at[pl.ds(0, experts - 1)], w_sem.at[0])
     sent(ds.at[pl.ds(0, experts - 1)], d_sem.at[0])
-    sent(xs.at[pl.ds(0, experts - 1)], t_send.at[0])
-    sent(rs.at[pl.ds(0, experts - 1)], r_sem.at[0])
+    sent(xs.at[pl.ds(0, GROUP - 1)], t_send.at[0])
+    for f in range(groups - 1):
+        for copy in to_door(f):
+            copy.wait_send()
+
+    @pl.when(is_door == 1)
+    def _():
+        sent(rb.at[pl.ds(0, 6 * (GROUP - 1))], rb_send.at[0])
+        sent(mb, mb_send.at[0])
+        sent(rs.at[pl.ds(0, experts - 7)], r_sem.at[0])
+
+    @pl.when(is_door == 0)
+    def _():
+        sent(rs.at[pl.ds(0, experts - 1)], r_sem.at[0])
+
     y_gu.wait_send()
     y_down.wait_send()
     for j in range(1, tps):
@@ -336,15 +501,16 @@
 
 
 def finish(
-    gate_h, up_h, down_h, rt_h, sel_h, wts_h,
+    gate_h, up_h, down_h, near_h, far_h, sel_h, wts_h,
     gate_o, up_o, down_o, mixed_o,
-    gate, up, down, rt, sel, wts, flat, mixed, in_sem, out_sem,
+    gate, up, down, rt, far, sel, wts, flat, mixed, in_sem, out_sem,
 ):
-    experts, cap, _width = rt.shape
+    near, cap, _width = rt.shape
+    many = far.shape[1]
     loads = [
         pltpu.make_async_copy(src, dst, in_sem.at[k])
         for k, (src, dst) in enumerate(
-            ((rt_h, rt), (sel_h, sel), (wts_h, wts), (gate_h, gate), (up_h, up), (down_h, down))
+            ((near_h, rt), (far_h, far), (sel_h, sel), (wts_h, wts), (gate_h, gate), (up_h, up), (down_h, down))
         )
     ]
     for load in loads:
@@ -357,12 +523,15 @@
         flat[at] = jnp.concatenate(two, axis=0).astype(BF16)
         return 0
 
-    lax.fori_loop(0, experts // 2, pair, 0)
+    lax.fori_loop(0, near // 2, pair, 0)
     loads[1].wait()
+    for f in range(far.shape[0]):
+        flat[near * cap + f * many : near * cap + (f + 1) * many] = far[f]
     loads[2].wait()
+    loads[3].wait()
     stores = []
     for k, (src, dst) in enumerate(((gate, gate_o), (up, up_o), (down, down_o))):
-        loads[3 + k].wait()
+        loads[4 + k].wait()
         stores.append(pltpu.make_async_copy(src, dst, out_sem.at[k]))
         stores[-1].start()
     parts = 2
@@ -386,6 +555,9 @@
     hid = down_master.shape[1]
     span = experts // tps
     block = experts // CHUNKS * cap
+    groups = experts // GROUP
+    many = GROUP * cap // top
+    all_rows = GROUP * cap + (groups - 1) * many
     dma = pltpu.SemaphoreType.DMA
     vmem = pltpu.VMEM
     spec_v = pl.BlockSpec(memory_space=pltpu.VMEM)
@@ -396,12 +568,13 @@
             jax.ShapeDtypeStruct((experts, depth, ff), BF16),
             jax.ShapeDtypeStruct((experts, depth, ff), BF16),
             jax.ShapeDtypeStruct((span, hid, width * tps), BF16),
-            jax.ShapeDtypeStruct((experts, cap, width), BF16),
-            jax.ShapeDtypeStruct((top, rows, experts * cap), BF16),
+            jax.ShapeDtypeStruct((GROUP, cap, width), BF16),
+            jax.ShapeDtypeStruct((groups - 1, many, width), BF16),
+            jax.ShapeDtypeStruct((top, rows, all_rows), BF16),
             jax.ShapeDtypeStruct((rows, 128), F32),
         ),
         in_specs=[spec_a, spec_v, spec_a, spec_a, spec_a, spec_v, spec_v],
-        out_specs=[spec_a] * 6,
+        out_specs=[spec_a] * 7,
         scratch_shapes=[
             vmem((rows, width), BF16),
             vmem((experts, depth, ff), F32),
@@ -412,17 +585,32 @@
             vmem((2, tps - 1, span, depth, ff), BF16),
             vmem((experts, hid, width), BF16),
             vmem((rows, width), BF16),
-            vmem((experts, cap, width), BF16),
+            vmem((GROUP, cap, width), BF16),
+            vmem((groups - 1, many, width), BF16),
+            vmem((groups - 1, 8, 128), F32),
             vmem((experts, cap, width), BF16),
             vmem((block, width), BF16),
-            vmem((CHUNKS, tps - 1, block, 2 * ff), F32),
-            vmem((CHUNKS, tps - 1, block, 2 * ff), F32),
-            vmem((block, 2 * ff), F32),
+            vmem((CHUNKS, tps - 1, block, 2 * ff), BF16),
+            vmem((CHUNKS, tps - 1, block, 2 * ff), BF16),
+            vmem((CHUNKS, block, 2 * ff), F32),
             vmem((CHUNKS, tps, block, ff), BF16),
             vmem((experts, cap, width), BF16),
-            vmem((top, rows, experts * cap), BF16),
+            vmem((top, rows, all_rows), BF16),
             vmem((rows, 128), F32),
             vmem((tps, rows, 128), F32),
+            vmem((6, many, width), BF16),
+            vmem((6, 8, 128), F32),
+            vmem((6 * GROUP, cap, width), BF16),
+            vmem((6 * GROUP, cap, width), BF16),
+            vmem((6, many, width), BF16),
+            dma((groups - 1,)),
+            dma((6,)),
+            dma((groups - 1,)),
+            dma((6,)),
+            dma((1,)),
+            dma((6,)),
+            dma((1,)),
+            dma((groups - 1,)),
             dma((3,)),
             dma((2,)),
             dma((2,)),
@@ -454,14 +642,14 @@
             *(jax.ShapeDtypeStruct(shape, BF16) for shape in shapes[:3]),
             jax.ShapeDtypeStruct((rows, width), BF16),
         ),
-        in_specs=[spec_a] * 6,
+        in_specs=[spec_a] * 7,
         out_specs=[spec_a] * 4,
         scratch_shapes=[
-            *(vmem(shape, BF16) for shape in shapes[:5]),
-            vmem(shapes[5], F32),
-            vmem((experts * cap, width), BF16),
+            *(vmem(shape, BF16) for shape in shapes[:6]),
+            vmem(shapes[6], F32),
+            vmem((all_rows, width), BF16),
             vmem((rows, width), BF16),
-            dma((6,)),
+            dma((7,)),
             dma((5,)),
         ],
         compiler_params=pltpu.CompilerParams(vmem_limit_bytes=60 * 1024 * 1024),

time: 238 us -> 227 us (0.954)
  Pallas kernels: 237 us -> 226 us
    pallas_call x1, Pallas kernels: 232 us -> 222 us  [shards(): pl.pallas_call(functools.partial(kernel, (experts, tps, rows, top, cap)),...]
where the time goes in v4:
time: 227 us
  Pallas kernels  226 us (100%)
    pallas_call x1, Pallas kernels, shards(): pl.pallas_call(functools.partial(kernel, (experts, tps, rows, top, cap)),...  222 us

profile of v4, /device:TPU:33, one launch (start us, length us, event | category | flops | bytes accessed | tf_op | source)
XLA Modules:
  0.0 227.1 jit_solution(13752942161367492017)
XLA Ops:
  0.6 222.1 %shard_map.102 = (bf16[32,128,128]{2,1,0:T(8,128)(2,1)}, bf16[32,128,128]{2,1,0:T(8,128)(2,1)}, bf16[8,16,4096]{2,1,0:T(8,128)(2,1)}, bf16[8,24,1024]{2,1,0:T(8,...) custom-call(bf16[384,1024]{1,0:T(8,128)(2,1)} %tok_h.1, ...), custom_call_target="tpu_custom_call" | custom-call | tf_op jit(solution)/shard_map/pallas_call | solution.py:565
  222.8 4.3 %shard_map.103 = (bf16[32,128,128]{2,1,0:T(8,128)(2,1)}, bf16[32,128,128]{2,1,0:T(8,128)(2,1)}, bf16[8,16,4096]{2,1,0:T(8,128)(2,1)}, bf16[384,1024]{1,0:T(8,128)(2,1)}) custom-call(bf16[32,128,128]{2,1,0:T(8,128)(2,1)} %get-tuple-element.15.gate_h, bf16[32,128,128]{2,1,0:T(8,128)(2,1)} %get-tuple-element.16.up_h, ...), custom_call_target="tpu_custom_call" | custom-call | tf_op jit(solution)/shard_map/pallas_call | solution.py:639

commit v5 on v4

--- a/solution.py
+++ b/solution.py
@@ -24,6 +24,10 @@
     peer = 2 * ((z + dz + rings) % rings) + (core + other) % 2
     inner = ((n + rings - 1) // rings) * (1 - n // (rings - 1))
     return peer, 2 * (n + sign * inner) + m % 2
+
+
+def door_of(way, core):
+    return way * (6 - core) + (1 - way) * 3 * core
 
 
 def classes(shape, axis, home, groups):
@@ -92,7 +96,8 @@
     other = 2 * z + 1 - core
     home, mine = fs // GROUP, fs % GROUP
     pos = mine // 2
-    is_door = 1 - (pos + 1) // 2 % 2
+    inner = (pos + 1) // 2 % 2
+    is_door = inner * core + (1 - inner) * (1 - core)
     side = grp % 2
     partner = grp + 1 - 2 * side
     width = tok.shape[1]
@@ -217,9 +222,9 @@
     turn = pos // 2
     hops = (4 - pos, pos + 1, turn * (8 - pos) + (1 - turn) * (pos + 5))
     doors = (
-        GROUP * ((home + 1) % groups) + core,
-        GROUP * ((home + 3) % groups) + GROUP - 2 + core,
-        GROUP * ((home + 2) % groups) + (GROUP - 2) * (1 - turn) + core,
+        GROUP * ((home + 1) % groups) + door_of(0, core),
+        GROUP * ((home + 3) % groups) + door_of(1, core),
+        GROUP * ((home + 2) % groups) + door_of(1 - turn, core),
     )
 
     def to_door(f):
@@ -300,7 +305,7 @@
             out = out + jnp.dot(two[1], flat, preferred_element_type=F32) * turned[:, 3:4]
             mb[i] = out.astype(BF16)
             f = turn if i < 4 else 2
-            back_to = (z + (2 * turn - 1) * (i + 1) + rings) % rings
+            back_to = (z + (2 * turn - 1) * (i + 1 + core) + rings) % rings
             remote(mb.at[i], rt_far.at[f], mb_send.at[0], far_recv.at[f], {"fs": 2 * back_to + core}).start()
 
     def forward(phase, q):
@@ -421,7 +426,7 @@
 
             def back(k, _):
                 i = 5 - (2 * (ch - 1) + k // 4)
-                door = GROUP * home + (GROUP - 2) * (k % 4 // 2) + k % 2
+                door = GROUP * home + door_of(k % 4 // 2, k % 2)
                 spot = i * GROUP + mine
 
                 @pl.when(door == fs)
@@ -447,15 +452,19 @@
     activate(2)
     contract(0)
     project(2)
+    hand_back(5)
+    hand_back(4)
     contract(3)
+    activate(3)
+    hand_back(3)
+    project(3)
     activate(0)
-    activate(3)
+    hand_back(2)
     project(0)
-    project(3)
     for j in range(1, tps):
         down_send(j).start()
     down_own.start()
-    for i in range(5, -1, -1):
+    for i in range(1, -1, -1):
         hand_back(i)
     own_back = pltpu.make_async_copy(rs.at[mine], rt_near.at[mine], o_sem.at[3])
     own_back.start()

time: 227 us -> 217 us (0.956)
  Pallas kernels: 226 us -> 216 us
    pallas_call x1, Pallas kernels: 222 us -> 212 us  [shards(): pl.pallas_call(functools.partial(kernel, (experts, tps, rows, top, cap)),...]
where the time goes in v5:
time: 217 us
  Pallas kernels  216 us (100%)
    pallas_call x1, Pallas kernels, shards(): pl.pallas_call(functools.partial(kernel, (experts, tps, rows, top, cap)),...  212 us

profile of v5, /device:TPU:33, one launch (start us, length us, event | category | flops | bytes accessed | tf_op | source)
XLA Modules:
  0.0 216.8 jit_solution(12006684102426237478)
XLA Ops:
  0.6 211.8 %shard_map.102 = (bf16[32,128,128]{2,1,0:T(8,128)(2,1)}, bf16[32,128,128]{2,1,0:T(8,128)(2,1)}, bf16[8,16,4096]{2,1,0:T(8,128)(2,1)}, bf16[8,24,1024]{2,1,0:T(8,...) custom-call(bf16[384,1024]{1,0:T(8,128)(2,1)} %tok_h.1, ...), custom_call_target="tpu_custom_call" | custom-call | tf_op jit(solution)/shard_map/pallas_call | solution.py:574
  212.4 4.3 %shard_map.103 = (bf16[32,128,128]{2,1,0:T(8,128)(2,1)}, bf16[32,128,128]{2,1,0:T(8,128)(2,1)}, bf16[8,16,4096]{2,1,0:T(8,128)(2,1)}, bf16[384,1024]{1,0:T(8,128)(2,1)}) custom-call(bf16[32,128,128]{2,1,0:T(8,128)(2,1)} %get-tuple-element.15.gate_h, bf16[32,128,128]{2,1,0:T(8,128)(2,1)} %get-tuple-element.16.up_h, ...), custom_call_target="tpu_custom_call" | custom-call | tf_op jit(solution)/shard_map/pallas_call | solution.py:648

commit v6 on v5

--- a/solution.py
+++ b/solution.py
@@ -445,16 +445,16 @@
     y_down = remote(dr.at[:, :, my_cols], dr.at[:, :, my_cols], y_send.at[1], y_recv.at[1], {"grp": partner})
     y_down.start()
     contract(1)
+    contract(2)
     activate(1)
     y_down.wait_recv()
     project(1)
-    contract(2)
     activate(2)
     contract(0)
     project(2)
+    contract(3)
     hand_back(5)
     hand_back(4)
-    contract(3)
     activate(3)
     hand_back(3)
     project(3)

time: 217 us -> 211 us (0.972)
  Pallas kernels: 216 us -> 209 us
    pallas_call x1, Pallas kernels: 212 us -> 205 us  [shards(): pl.pallas_call(functools.partial(kernel, (experts, tps, rows, top, cap)),...]
where the time goes in v6:
time: 211 us; the launch traced here: 210 us
  Pallas kernels  209 us (99%)
    pallas_call x1, Pallas kernels, shards(): pl.pallas_call(functools.partial(kernel, (experts, tps, rows, top, cap)),...  205 us
    pallas_call x1, Pallas kernels, shards(): pl.pallas_call(finish, out_shape=(*(jax.ShapeDtypeStruct(shape, BF16) for...  4.32 us

profile of v6, /device:TPU:33, one launch (start us, length us, event | category | flops | bytes accessed | tf_op | source)
XLA Modules:
  0.0 209.6 jit_solution(6413068385341317080)
XLA Ops:
  0.6 204.7 %shard_map.102 = (bf16[32,128,128]{2,1,0:T(8,128)(2,1)}, bf16[32,128,128]{2,1,0:T(8,128)(2,1)}, bf16[8,16,4096]{2,1,0:T(8,128)(2,1)}, bf16[8,24,1024]{2,1,0:T(8,...) custom-call(bf16[384,1024]{1,0:T(8,128)(2,1)} %tok_h.1, ...), custom_call_target="tpu_custom_call" | custom-call | tf_op jit(solution)/shard_map/pallas_call | solution.py:574
  205.3 4.3 %shard_map.103 = (bf16[32,128,128]{2,1,0:T(8,128)(2,1)}, bf16[32,128,128]{2,1,0:T(8,128)(2,1)}, bf16[8,16,4096]{2,1,0:T(8,128)(2,1)}, bf16[384,1024]{1,0:T(8,128)(2,1)}) custom-call(bf16[32,128,128]{2,1,0:T(8,128)(2,1)} %get-tuple-element.15.gate_h, bf16[32,128,128]{2,1,0:T(8,128)(2,1)} %get-tuple-element.16.up_h, ...), custom_call_target="tpu_custom_call" | custom-call | tf_op jit(solution)/shard_map/pallas_call | solution.py:648
